TPU v7x, 32 devices: a whole 2x2x4 slice. The times are simulated.
32 devices in a mesh: sp: 8 (over z, y), tp: 4 (over x, core).
Axes of the slice: x: 2, y: 2, z: 4, core: 2. Of those that a mesh axis runs over, the one named last changes fastest.
Arguments:
- residual: bfloat16 [6144, 2048], P(('sp', 'tp')), may hold values from -6 to 6
- queries: bfloat16 [6144, 1024], P('sp', 'tp'), may hold values from -240 to 240
- keys: bfloat16 [6144, 256], P('sp', 'tp'), may hold values from -6 to 6
- values: bfloat16 [6144, 256], P('sp', 'tp'), may hold values from -18 to 18
- sinks: float32 [16], P('tp'), may hold values from 1 to 6
- out_weight: bfloat16 [1024, 2048], replicated, may hold values from -0.5625 to 0.5625
- norm_gain: float32 [2048], replicated, may hold values from 0.1 to 1.9
- gate_weight: bfloat16 [2048, 5632], P('sp', 'tp'), may hold values from -0.125 to 0.125
- up_weight: bfloat16 [2048, 5632], P('sp', 'tp'), may hold values from -0.125 to 0.125
- down_weight: bfloat16 [5632, 2048], P('tp', 'sp'), may hold values from -0.078125 to 0.078125
Outputs:
- layer_out: bfloat16 [6144, 2048], P(('sp', 'tp'))
All inputs are finite; a program needn't handle non-finite values.
Results may differ from a plain program's by a relative error of at most 0.014.
Values may be sent and summed in bfloat16 or wider, within the bound.
No kernel may reach another device: no remote copies, remote signals or barrier semaphores. Data moves between devices by JAX's collectives and lax.ppermute only.
A program may use at most 128 MiB of HBM per device.

v0:
```python
import jax
import jax.numpy as jnp
from jax import lax
from jax.sharding import PartitionSpec as P

HEAD = 64
WINDOW = 128


def passed_along(block, axis, distance):
    devices = range(lax.axis_size(axis))
    route = [(i - distance, i) for i in devices if i - distance in devices]
    return lax.ppermute(block, axis, route)


def attend(queries, keys_ext, values_ext, sinks, block_base):
    rows = queries.shape[0]
    nblk = rows // WINDOW
    qheads = sinks.shape[0]
    kheads = keys_ext.shape[1] // HEAD
    group = qheads // kheads
    qblock = queries.reshape(nblk, WINDOW, kheads, group, HEAD).astype(jnp.float32)

    def band(arr):
        first = arr[:rows].reshape(nblk, WINDOW, kheads, HEAD)
        second = arr[WINDOW:].reshape(nblk, WINDOW, kheads, HEAD)
        return jnp.concatenate([first, second], axis=1).astype(jnp.float32)

    kband = band(keys_ext)
    vband = band(values_ext)
    score = jnp.einsum("nqhgd,nkhd->nhgqk", qblock, kband) * HEAD ** (-0.5)
    qidx = jnp.arange(WINDOW)[:, None]
    kidx = jnp.arange(2 * WINDOW)[None, :]
    rel = qidx + WINDOW - kidx
    valid = (rel >= 0) & (rel < WINDOW)
    blocks = block_base + jnp.arange(nblk)
    valid = valid[None] & ((blocks > 0)[:, None, None] | (kidx >= WINDOW)[None])
    score = jnp.where(valid[:, None, None], score, -jnp.inf)
    sink = sinks.reshape(kheads, group)[None, :, :, None]
    top = jnp.maximum(jnp.max(score, axis=-1), sink)
    expd = jnp.exp(score - top[..., None])
    denom = jnp.sum(expd, axis=-1) + jnp.exp(sink - top)
    weights = (expd / denom[..., None]).astype(jnp.bfloat16)
    result = jnp.einsum("nhgqk,nkhd->nqhgd", weights.astype(jnp.float32), vband)
    return result.reshape(rows, qheads * HEAD).astype(jnp.bfloat16)


def shards(
    residual,
    queries,
    keys,
    values,
    sinks,
    out_weight,
    norm_gain,
    gate_weight,
    up_weight,
    down_weight,
):
    rows_dev = queries.shape[0]
    prev_keys, prev_values = passed_along((keys[-WINDOW:], values[-WINDOW:]), "sp", 1)
    keys_ext = jnp.concatenate([prev_keys, keys], axis=0)
    values_ext = jnp.concatenate([prev_values, values], axis=0)
    attention = attend(
        queries, keys_ext, values_ext, sinks, lax.axis_index("sp") * (rows_dev // WINDOW)
    )
    width = attention.shape[1]
    mine = lax.dynamic_slice_in_dim(out_weight, lax.axis_index("tp") * width, width, 0)
    proj = lax.psum_scatter(
        jnp.dot(attention, mine, preferred_element_type=jnp.float32).astype(jnp.bfloat16),
        "tp",
        scatter_dimension=0,
        tiled=True,
    ).astype(jnp.float32)
    mixed = (residual.astype(jnp.float32) + proj).astype(jnp.bfloat16)
    mixf = mixed.astype(jnp.float32)
    normed = (
        mixf * lax.rsqrt(jnp.mean(mixf * mixf, axis=-1, keepdims=True) + 1e-06) * norm_gain
    ).astype(jnp.bfloat16)
    normed_all = lax.all_gather(normed, "tp", axis=0, tiled=True)
    gate = jnp.dot(
        normed_all,
        lax.all_gather(gate_weight, "sp", axis=0, tiled=True),
        preferred_element_type=jnp.float32,
    )
    upper = jnp.dot(
        normed_all,
        lax.all_gather(up_weight, "sp", axis=0, tiled=True),
        preferred_element_type=jnp.float32,
    )
    hidden = (jax.nn.silu(gate) * upper).astype(jnp.bfloat16)
    terms = jnp.dot(
        hidden,
        lax.all_gather(down_weight, "sp", axis=1, tiled=True),
        preferred_element_type=jnp.float32,
    )
    ffn = lax.psum_scatter(
        terms.astype(jnp.bfloat16), "tp", scatter_dimension=0, tiled=True
    ).astype(jnp.float32)
    return (mixed.astype(jnp.float32) + ffn).astype(jnp.bfloat16)


def solution(mesh):
    placed = (
        P(("sp", "tp"), None),
        P("sp", "tp"),
        P("sp", "tp"),
        P("sp", "tp"),
        P("tp"),
        P(),
        P(),
        P("sp", "tp"),
        P("sp", "tp"),
        P("tp", "sp"),
    )
    return jax.shard_map(
        shards, mesh=mesh, in_specs=placed, out_specs=P(("sp", "tp"), None), check_vma=False
    )
```

profile of v0, /device:TPU:0, one launch (start us, length us, event | category | flops | bytes accessed | tf_op | source)
XLA Modules:
  0.0 407.9 jit_solution(3157988359120101178)
XLA Ops:
  7.4 0.0 reduce-scatter.3.cloned.1.call-start
  7.4 0.7 slice.14
  8.1 4.9 %collective-permute-start.1 = (bf16[128,64]{0,1:T(8,128)(2,1)S(1)}, bf16[128,64]{0,1:T(8,128)(2,1)S(1)}, u32[]{:S(2)}, u32[]{:S(2)}) collective-permute-start(bf16[128,64]{0,1:T(8,128)(2,1)S(1)} %slice.14), channel_id=1, source_target_pairs={{0,4},{4,8},{8,12},{12,16},{16,20},{20,24},{24,28},{1,5},{5,9},{9,... | collective-permute-start | bytes 49160 | tf_op jit(solution)/shard_map/ppermute | solution.py:13
  13.0 0.7 slice.12
  13.7 3.4 collective-permute-start
  17.2 0.1 broadcast_or_fusion
  17.3 0.3 broadcast_and_fusion
  17.6 1.0 reshape.145
  18.6 1.0 reshape.142
  19.6 0.0 copy-start.4
  19.6 2.5 reshape.151
  22.2 0.6 copy.14
  22.9 0.0 collective-permute-done.1
  22.9 0.9 pad_maximum_fusion
  23.8 0.1 reshape.144
  23.9 0.0 copy-start.2
  23.9 1.9 fusion.1
  25.8 0.0 copy-done.4
  25.8 0.1 broadcast_maximum_fusion
  25.9 0.7 fusion
  26.6 0.1 exponential_add_fusion
  26.7 0.0 collective-permute-done
  26.7 0.0 copy-done.2
  26.7 0.7 pad_maximum_fusion.1
  27.3 1.0 reshape.141
  28.4 1.8 fusion.12
  30.2 0.3 copy.20
  30.5 4.0 convolution_convert_fusion
  34.5 0.0 copy-start
  34.5 0.0 copy-start.3
  34.5 0.0 reduce-scatter.3.cloned.1.call-update
  34.5 0.0 all-gather.7.cloned.1.call-start
  34.6 0.5 all-gather.7.cloned.1.call-update
  35.1 0.0 all-gather.5.cloned.1.call-start
  35.1 37.7 %reduce-scatter.3.cloned.1.call-done = bf16[192,2048]{1,0:T(8,128)(2,1)} async-done(((bf16[768,2048]{1,0:T(8,128)(2,1)}), bf16[192,2048]{1,0:T(8,128)(2,1)}) %reduce-scatter.3.cloned.1.call-update) | async-done | bytes 786448 | tf_op jit(solution)/shard_map/reduce_scatter | solution.py:69
  72.8 0.0 copy-done
  72.8 1.5 fusion.2
  74.3 0.0 copy-done.3
  74.3 2.3 fusion.4
  76.6 0.0 all-gather.5.cloned.1.call-update
  76.6 0.0 all-gather.11.cloned.1.call-start
  76.7 0.5 all-gather.11.cloned.1.call-update
  77.2 0.0 all-gather.9.cloned.1.call-start
  77.3 0.7 all-gather.9.cloned.1.call-update
  77.9 0.2 reduce-scatter.5.cloned.1.call-start
  78.2 51.4 %all-gather.7.cloned.1.call-done = bf16[2048,1408]{1,0:T(8,128)(2,1)} async-done(((bf16[256,1408]{1,0:T(8,128)(2,1)}), bf16[2048,1408]{1,0:T(8,128)(2,1)}) %all-gather.7.cloned.1.call-update) | async-done | bytes 5767184 | tf_op jit(solution)/shard_map/all_gather | solution.py:83
  129.6 28.0 %all-gather.5.cloned.1.call-done = bf16[768,2048]{1,0:T(8,128)(2,1)} async-done(((bf16[192,2048]{1,0:T(8,128)(2,1)}), bf16[768,2048]{1,0:T(8,128)(2,1)}) %all-gather.5.cloned.1.call-update) | async-done | bytes 3145744 | tf_op jit(solution)/shard_map/all_gather | solution.py:80
  157.6 9.7 %fusion.33 = f32[768,1408]{1,0:T(8,128)} fusion(bf16[768,2048]{1,0:T(8,128)(2,1)} %all-gather.5.cloned.1.call-done, bf16[2048,1408]{1,0:T(8,128)(2,1)} %all-gather.7.cloned.1.call-done), kind=kOutput, calls=%fused_computation.52 | convolution fusion | flops 4429185024 | bytes 13238272 | tf_op jit(solution)/shard_map/dot_general | solution.py:81
  167.2 85.1 %all-gather.11.cloned.1.call-done = bf16[1408,2048]{1,0:T(8,128)(2,1)} async-done(((bf16[1408,256]{1,0:T(8,128)(2,1)}), bf16[1408,2048]{1,0:T(8,128)(2,1)}) %all-gather.11.cloned.1.call-update) | async-done | bytes 5767184 | tf_op jit(solution)/shard_map/all_gather | solution.py:94
  252.4 92.5 %all-gather.9.cloned.1.call-done = bf16[2048,1408]{1,0:T(8,128)(2,1)} async-done(((bf16[256,1408]{1,0:T(8,128)(2,1)}), bf16[2048,1408]{1,0:T(8,128)(2,1)}) %all-gather.9.cloned.1.call-update) | async-done | bytes 5767184 | tf_op jit(solution)/shard_map/all_gather | solution.py:88
  344.9 16.8 %convolution_convert_fusion.1 = bf16[768,2048]{1,0:T(8,128)(2,1)} fusion(bf16[1408,2048]{1,0:T(8,128)(2,1)} %all-gather.11.cloned.1.call-done, f32[768,1408]{1,0:T(8,128)} %fusion.33, bf16[768,2048]{1,0:T(8,128)(2,1)} %all-gather.5.cloned.1.call-done, bf16[2048,1408]{1,0:T(8,128)(2,1)} %all-gather.9.cloned.1.call-done), kind=kOutput, calls=%fused_computation.2 | convolution fusion | flops 8866430976 | bytes 22151168 | tf_op jit(solution)/shard_map/dot_general | solution.py:92
  361.7 0.0 copy-start.1
  361.7 0.0 reduce-scatter.5.cloned.1.call-update
  361.7 36.2 %reduce-scatter.5.cloned.1.call-done = bf16[192,2048]{1,0:T(8,128)(2,1)} async-done(((bf16[768,2048]{1,0:T(8,128)(2,1)}), bf16[192,2048]{1,0:T(8,128)(2,1)}) %reduce-scatter.5.cloned.1.call-update) | async-done | bytes 786448 | tf_op jit(solution)/shard_map/reduce_scatter | solution.py:97
  397.9 0.0 copy-done.1
  397.9 2.4 fusion.5
  (8 shorter events, 0.1 us)
Async XLA Ops:
  7.4 65.4 %reduce-scatter.3.cloned.1.call-start = ((), (), s32[]{:S(2)}) async-start(), calls=%async_computation.2 | async-start | bytes 3932160 | tf_op jit(solution)/shard_map/reduce_scatter | solution.py:69
  8.1 14.8 %collective-permute-start.1 = (bf16[128,64]{0,1:T(8,128)(2,1)S(1)}, bf16[128,64]{0,1:T(8,128)(2,1)S(1)}, u32[]{:S(2)}, u32[]{:S(2)}) collective-permute-start(bf16[128,64]{0,1:T(8,128)(2,1)S(1)} %slice.14), channel_id=1, source_target_pairs={{0,4},{4,8},{8,12},{12,16},{16,20},{20,24},{24,28},{1,5},{5,9},{9,... | collective-permute-start | bytes 49160 | tf_op jit(solution)/shard_map/ppermute | solution.py:13
  13.7 13.0 %collective-permute-start = (bf16[128,64]{0,1:T(8,128)(2,1)S(1)}, bf16[128,64]{0,1:T(8,128)(2,1)S(1)}, u32[]{:S(2)}, u32[]{:S(2)}) collective-permute-start(bf16[128,64]{0,1:T(8,128)(2,1)S(1)} %slice.12), channel_id=1, source_target_pairs={{0,4},{4,8},{8,12},{12,16},{16,20},{20,24},{24,28},{1,5},{5,9},{9,... | collective-permute-start | bytes 49160 | tf_op jit(solution)/shard_map/ppermute | solution.py:13
  19.6 6.2 %copy-start.4 = (f32[4]{0:T(128)S(1)}, f32[4]{0:T(128)}, u32[]{:S(2)}) copy-start(f32[4]{0:T(128)} %param.14) | copy-start | bytes 52
  23.9 2.8 copy-start.2
  34.5 38.3 %copy-start = (bf16[192,2048]{1,0:T(8,128)(2,1)S(1)}, bf16[192,2048]{1,0:T(8,128)(2,1)}, u32[]{:S(2)}) copy-start(bf16[192,2048]{1,0:T(8,128)(2,1)} %param.10) | copy-start | bytes 2359300
  34.5 39.8 %copy-start.3 = (f32[2048]{0:T(1024)S(1)}, f32[2048]{0:T(1024)}, u32[]{:S(2)}) copy-start(f32[2048]{0:T(1024)} %param.16) | copy-start | bytes 24580
  34.5 95.1 %all-gather.7.cloned.1.call-start = ((), (), s32[]{:S(2)}) async-start(), calls=%async_computation.4 | async-start | bytes 6488064 | tf_op jit(solution)/shard_map/all_gather | solution.py:83
  35.1 122.5 %all-gather.5.cloned.1.call-start = ((), (), s32[]{:S(2)}) async-start(), calls=%async_computation.3 | async-start | bytes 3932160 | tf_op jit(solution)/shard_map/all_gather | solution.py:80
  76.6 175.8 %all-gather.11.cloned.1.call-start = ((), (), s32[]{:S(2)}) async-start(), calls=%async_computation.6 | async-start | bytes 6488064 | tf_op jit(solution)/shard_map/all_gather | solution.py:94
  77.2 267.7 %all-gather.9.cloned.1.call-start = ((), (), s32[]{:S(2)}) async-start(), calls=%async_computation.5 | async-start | bytes 6488064 | tf_op jit(solution)/shard_map/all_gather | solution.py:88
  77.9 320.0 %reduce-scatter.5.cloned.1.call-start = ((), (), s32[]{:S(2)}) async-start(), calls=%async_computation.7 | async-start | bytes 3932160 | tf_op jit(solution)/shard_map/reduce_scatter | solution.py:97
  361.7 36.2 %copy-start.1 = (bf16[192,2048]{1,0:T(8,128)(2,1)S(1)}, bf16[192,2048]{1,0:T(8,128)(2,1)}, u32[]{:S(2)}) copy-start(bf16[192,2048]{1,0:T(8,128)(2,1)} %reduce-scatter.3.cloned.1.call-done) | copy-start | bytes 2359300
Sparse Core Ops, SparseCore 0:
  34.6 38.1 reduce-scatter.2
  361.9 35.9 reduce-scatter.4
Sparse Core Ops, SparseCore 1:
  37.2 92.4 all-gather.6
  131.0 26.5 all-gather.4
  159.5 92.9 all-gather.10
  254.6 90.3 all-gather.8
where the time goes:
time: 409 us; the launch traced here: 408 us
  waiting for transfers between devices  333 us (81%)
  matrix products  34.1 us (8%)
  between operations  15.2 us (4%)
  other arithmetic  8.99 us (2%)
  starting transfers between devices  8.7 us (2%)
  local copies, waits for them, and re-layouts  8.18 us (2%)
    all_gather x1, waiting for transfers between devices, shards(): lax.all_gather(up_weight, 'sp', axis=0, tiled=True)  92.5 us
    all_gather x1, waiting for transfers between devices, shards(): lax.all_gather(down_weight, 'sp', axis=1, tiled=True)  85.1 us
    all_gather x1, waiting for transfers between devices, shards(): lax.all_gather(gate_weight, 'sp', axis=0, tiled=True)  51.4 us
    reduce_scatter x1, waiting for transfers between devices, shards(): lax.psum_scatter(jnp.dot(attention, mine, preferred_element_type=jnp.floa...  37.7 us
    reduce_scatter x1, waiting for transfers between devices, shards(): lax.psum_scatter(terms.astype(jnp.bfloat16), 'tp', scatter_dimension=0, t...  36.2 us
    all_gather x1, waiting for transfers between devices, shards(): normed_all = lax.all_gather(normed, 'tp', axis=0, tiled=True)  28 us
    dot_general x1, matrix products, shards(): jnp.dot(hidden, lax.all_gather(down_weight, 'sp', axis=1, tiled=True), pr...  16.8 us
    dot_general x1, matrix products, shards(): jnp.dot(normed_all, lax.all_gather(gate_weight, 'sp', axis=0, tiled=True)...  9.69 us
  transfers between devices with their start and end apart: 8, of which 6 were waited for; matrix products, arithmetic and copies ran while one was open for 6% of the time, Pallas kernels for 0%

commit v1 on v0

--- a/solution.py
+++ b/solution.py
@@ -3,8 +3,10 @@
 from jax import lax
 from jax.sharding import PartitionSpec as P
 
+
 HEAD = 64
 WINDOW = 128
+LANES = 128
 
 
 def passed_along(block, axis, distance):
@@ -45,6 +47,43 @@
     return result.reshape(rows, qheads * HEAD).astype(jnp.bfloat16)
 
 
+def ring_order(count):
+    return list(range(0, count, 2)) + list(range(1, count, 2))[::-1]
+
+
+def uses_ring(count, widths):
+    return count > 1 and count % 2 == 0 and min(widths) >= LANES
+
+
+def ring_hops(shard, axis, dim):
+    count = lax.axis_size(axis)
+    if not uses_ring(count, (shard.shape[dim],)):
+        return [[(jnp.uint32(0), lax.all_gather(shard, axis, axis=dim, tiled=True))]]
+    order = ring_order(count)
+    place = [0] * count
+    for at, dev in enumerate(order):
+        place[dev] = at
+    table = [[order[(place[dev] + step) % count] for step in range(count)] for dev in range(count)]
+    owners = jnp.array(table, jnp.uint32)[lax.axis_index(axis)]
+    ahead = [(order[i], order[(i + 1) % count]) for i in range(count)]
+    back = [(dst, src) for src, dst in ahead]
+
+    def owner(step):
+        return owners[step % count]
+
+    hops = [[(owner(0), shard)]]
+    from_left = from_right = shard
+    for step in range(1, count // 2):
+        from_left = lax.ppermute(from_left, axis, ahead)
+        from_right = lax.ppermute(from_right, axis, back)
+        hops.append([(owner(-step), from_left), (owner(step), from_right)])
+    half = shard.shape[0] // 2
+    top = lax.ppermute(from_left[:half], axis, ahead)
+    bottom = lax.ppermute(from_right[half:], axis, back)
+    hops.append([(owner(count // 2), jnp.concatenate([top, bottom], axis=0))])
+    return hops
+
+
 def shards(
     residual,
     queries,
@@ -59,45 +98,53 @@
 ):
     rows_dev = queries.shape[0]
     prev_keys, prev_values = passed_along((keys[-WINDOW:], values[-WINDOW:]), "sp", 1)
+    gate_hops = ring_hops(gate_weight, "sp", 0)
+    up_hops = ring_hops(up_weight, "sp", 0)
+    down_hops = ring_hops(down_weight, "sp", 1)
+
     keys_ext = jnp.concatenate([prev_keys, keys], axis=0)
     values_ext = jnp.concatenate([prev_values, values], axis=0)
     attention = attend(
         queries, keys_ext, values_ext, sinks, lax.axis_index("sp") * (rows_dev // WINDOW)
     )
-    width = attention.shape[1]
-    mine = lax.dynamic_slice_in_dim(out_weight, lax.axis_index("tp") * width, width, 0)
-    proj = lax.psum_scatter(
-        jnp.dot(attention, mine, preferred_element_type=jnp.float32).astype(jnp.bfloat16),
-        "tp",
-        scatter_dimension=0,
-        tiled=True,
-    ).astype(jnp.float32)
+    attention = lax.all_to_all(attention, "tp", split_axis=0, concat_axis=1, tiled=True)
+    proj = jnp.dot(attention, out_weight, preferred_element_type=jnp.float32)
     mixed = (residual.astype(jnp.float32) + proj).astype(jnp.bfloat16)
     mixf = mixed.astype(jnp.float32)
     normed = (
         mixf * lax.rsqrt(jnp.mean(mixf * mixf, axis=-1, keepdims=True) + 1e-06) * norm_gain
     ).astype(jnp.bfloat16)
     normed_all = lax.all_gather(normed, "tp", axis=0, tiled=True)
-    gate = jnp.dot(
-        normed_all,
-        lax.all_gather(gate_weight, "sp", axis=0, tiled=True),
-        preferred_element_type=jnp.float32,
-    )
-    upper = jnp.dot(
-        normed_all,
-        lax.all_gather(up_weight, "sp", axis=0, tiled=True),
-        preferred_element_type=jnp.float32,
-    )
+
+    def contracted(hops):
+        total = None
+        for hop in hops:
+            for owner, block in hop:
+                depth = block.shape[0]
+                rows = lax.dynamic_slice_in_dim(normed_all, owner * depth, depth, 1)
+                part = jnp.dot(rows, block, preferred_element_type=jnp.float32)
+                total = part if total is None else total + part
+        return total
+
+    gate = contracted(gate_hops)
+    upper = contracted(up_hops)
     hidden = (jax.nn.silu(gate) * upper).astype(jnp.bfloat16)
-    terms = jnp.dot(
-        hidden,
-        lax.all_gather(down_weight, "sp", axis=1, tiled=True),
-        preferred_element_type=jnp.float32,
-    )
-    ffn = lax.psum_scatter(
-        terms.astype(jnp.bfloat16), "tp", scatter_dimension=0, tiled=True
-    ).astype(jnp.float32)
-    return (mixed.astype(jnp.float32) + ffn).astype(jnp.bfloat16)
+    groups = down_hops[1:]
+    groups = [down_hops[0] + groups[0]] + groups[1:] if groups else down_hops
+    out = mixed
+    for group in groups:
+        parts = [
+            jnp.dot(hidden, block, preferred_element_type=jnp.float32).astype(jnp.bfloat16)
+            for _, block in group
+        ]
+        terms = jnp.concatenate(parts, axis=1)
+        ffn = lax.psum_scatter(terms, "tp", scatter_dimension=0, tiled=True).astype(jnp.float32)
+        for at, (owner, block) in enumerate(group):
+            width = block.shape[1]
+            base = lax.dynamic_slice_in_dim(mixed, owner * width, width, 1).astype(jnp.float32)
+            piece = (base + ffn[:, at * width : (at + 1) * width]).astype(jnp.bfloat16)
+            out = lax.dynamic_update_slice_in_dim(out, piece, owner * width, 1)
+    return out
 
 
 def solution(mesh):

time: 409 us -> 362 us (0.89)
  waiting for transfers between devices: 333 us -> 166 us
  matrix products: 34.1 us -> 90.3 us
  starting transfers between devices: 8.7 us -> 39.5 us
  local copies, waits for them, and re-layouts: 8.18 us -> 19.2 us
  blocking collectives: 0 us -> 9.97 us
  other arithmetic: 8.99 us -> 17 us
    all_gather x3 -> x0, waiting for transfers between devices: 229 us -> none  [the longest x1 92.5 us: shards(): lax.all_gather(up_weight, 'sp', axis=0, tiled=True)]
    ppermute x0 -> x24, waiting for transfers between devices: none -> 98.3 us  [the longest x9 65.3 us: ring_hops(): from_left = lax.ppermute(from_left, axis, ahead)]
    dot_general x3 -> x25, matrix products: 30.4 us -> 85.8 us  [the longest x16 67.7 us: contracted(): part = jnp.dot(rows, block, preferred_element_type=jnp.float32)]
    ppermute x0 -> x24, starting transfers between devices: none -> 31 us  [the longest x9 14.3 us: ring_hops(): from_left = lax.ppermute(from_left, axis, ahead)]
    all_gather x1, waiting for transfers between devices: 28 us -> 0.01 us  [shards(): normed_all = lax.all_gather(normed, 'tp', axis=0, tiled=True)]
    all_to_all x0 -> x1, blocking collectives: none -> 9.97 us  [shards(): lax.all_to_all(attention, 'tp', split_axis=0, concat_axis=1, tiled=True)]
    dynamic_update_slice x0 -> x8, other arithmetic: none -> 7.13 us  [shards(): out = lax.dynamic_update_slice_in_dim(out, piece, owner * width, 1)]
    slice x0 -> x7, local copies, waits for them, and re-layouts: none -> 6.75 us  [the longest x3 3.54 us: ring_hops(): top = lax.ppermute(from_left[:half], axis, ahead)]
  transfers between devices with their start and end apart: 8 -> 31, of which waited for: 6 -> 15; matrix products, arithmetic and copies ran while one was open for 6% -> 30% of each run, Pallas kernels for 0% -> 0%
where the time goes in v1:
time: 362 us; the launch traced here: 361 us
  waiting for transfers between devices  166 us (46%)
  matrix products  90.3 us (25%)
  starting transfers between devices  39.5 us (11%)
  local copies, waits for them, and re-layouts  19.2 us (5%)
  between operations  18.6 us (5%)
  other arithmetic  17 us (5%)
  blocking collectives  9.97 us (3%)
    reduce_scatter x4, waiting for transfers between devices, shards(): lax.psum_scatter(terms, 'tp', scatter_dimension=0, tiled=True)  68 us
    dot_general x16, matrix products, contracted(): part = jnp.dot(rows, block, preferred_element_type=jnp.float32)  67.7 us
    ppermute x9, waiting for transfers between devices, ring_hops(): from_left = lax.ppermute(from_left, axis, ahead)  65.3 us
    ppermute x9, waiting for transfers between devices, ring_hops(): from_right = lax.ppermute(from_right, axis, back)  27.8 us
    dot_general x8, matrix products, shards(): jnp.dot(hidden, block, preferred_element_type=jnp.float32)  14.5 us
    ppermute x9, starting transfers between devices, ring_hops(): from_left = lax.ppermute(from_left, axis, ahead)  14.3 us
    all_to_all x1, blocking collectives, shards(): lax.all_to_all(attention, 'tp', split_axis=0, concat_axis=1, tiled=True)  9.97 us
    ppermute x9, starting transfers between devices, ring_hops(): from_right = lax.ppermute(from_right, axis, back)  9.46 us
  transfers between devices with their start and end apart: 31, of which 15 were waited for; matrix products, arithmetic and copies ran while one was open for 30% of the time, Pallas kernels for 0%

profile of v1, /device:TPU:0, one launch (start us, length us, event | category | flops | bytes accessed | tf_op | source)
XLA Modules:
  0.0 360.9 jit_solution(11273379039329084481)
XLA Ops:
  7.3 4.9 %collective-permute-start.1 = (bf16[128,64]{0,1:T(8,128)(2,1)S(1)}, bf16[128,64]{0,1:T(8,128)(2,1)S(1)}, u32[]{:S(2)}, u32[]{:S(2)}) collective-permute-start(bf16[128,64]{0,1:T(8,128)(2,1)S(1)} %slice.149), channel_id=1, source_target_pairs={{0,4},{4,8},{8,12},{12,16},{16,20},{20,24},{24,28},{1,5},{5,9},{9,... | collective-permute-start | bytes 49160 | tf_op jit(solution)/shard_map/ppermute | solution.py:15
  12.9 3.4 collective-permute-start
  18.8 2.5 reshape.251
  23.1 1.9 fusion.2
  27.6 2.6 fusion.12
  30.2 1.4 copy.68
  32.1 10.0 %all_to_all.16 = bf16[4,192,256]{2,1,0:T(8,128)(2,1)S(1)} all-to-all(bf16[4,192,256]{2,1,0:T(8,128)(2,1)S(1)} %reshape.252), channel_id=1, replica_groups=mesh['sp'=8,'tp'=4] {'tp'}, dimensions={0} | all-to-all | bytes 786432 | tf_op jit(solution)/shard_map/all_to_all | solution.py:110
  42.1 3.7 %fusion.3 = (f32[192]{0:T(256)S(1)}, bf16[192,2048]{1,0:T(8,128)(2,1)S(1)}) fusion(bf16[192,1024]{1,0:T(8,128)(2,1)S(1)} %bitcast.95, bf16[1024,2048]{1,0:T(8,128)(2,1)} %param.18, bf16[192,2048]{1,0:T(8,128)(2,1)} %param.13), kind=kOutput, calls=%fused_computation.10 | convolution fusion | flops 807665472 | bytes 6161152 | tf_op jit(solution)/shard_map/dot_general | solution.py:111
  47.0 1.6 collective-permute-start.2
  49.1 1.6 collective-permute-start.10
  51.1 1.5 collective-permute-start.19
  52.7 13.4 %collective-permute-done.2 = bf16[256,1408]{1,0:T(8,128)(2,1)S(1)} collective-permute-done((bf16[256,1408]{1,0:T(8,128)(2,1)S(1)}, bf16[256,1408]{1,0:T(8,128)(2,1)S(1)}, u32[]{:S(2)}, u32[]{:S(2)}) %collective-permute-start.2) | collective-permute-done | bytes 720928 | tf_op jit(solution)/shard_map/ppermute | solution.py:77
  66.1 1.6 collective-permute-start.18
  67.7 1.6 collective-permute-start.4
  69.3 12.3 %collective-permute-done.10 = bf16[256,1408]{1,0:T(8,128)(2,1)S(1)} collective-permute-done((bf16[256,1408]{1,0:T(8,128)(2,1)S(1)}, bf16[256,1408]{1,0:T(8,128)(2,1)S(1)}, u32[]{:S(2)}, u32[]{:S(2)}) %collective-permute-start.10) | collective-permute-done | bytes 720928 | tf_op jit(solution)/shard_map/ppermute | solution.py:77
  81.5 1.5 collective-permute-start.5
  83.1 1.6 collective-permute-start.12
  84.7 13.9 %collective-permute-done.19 = bf16[1408,256]{1,0:T(8,128)(2,1)S(1)} collective-permute-done((bf16[1408,256]{1,0:T(8,128)(2,1)}, bf16[1408,256]{1,0:T(8,128)(2,1)S(1)}, u32[]{:S(2)}, u32[]{:S(2)}) %collective-permute-start.19) | collective-permute-done | bytes 720928 | tf_op jit(solution)/shard_map/ppermute | solution.py:78
  99.0 1.5 collective-permute-start.21
  100.6 12.0 %collective-permute-done.4 = bf16[256,1408]{1,0:T(8,128)(2,1)} collective-permute-done((bf16[256,1408]{1,0:T(8,128)(2,1)S(1)}, bf16[256,1408]{1,0:T(8,128)(2,1)}, u32[]{:S(2)}, u32[]{:S(2)}) %collective-permute-start.4) | collective-permute-done | bytes 720928 | tf_op jit(solution)/shard_map/ppermute | solution.py:77
  112.5 1.6 collective-permute-start.20
  114.1 1.6 collective-permute-start.6
  115.7 12.3 %collective-permute-done.12 = bf16[256,1408]{1,0:T(8,128)(2,1)} collective-permute-done((bf16[256,1408]{1,0:T(8,128)(2,1)S(1)}, bf16[256,1408]{1,0:T(8,128)(2,1)}, u32[]{:S(2)}, u32[]{:S(2)}) %collective-permute-start.12) | collective-permute-done | bytes 720928 | tf_op jit(solution)/shard_map/ppermute | solution.py:77
  128.0 1.5 collective-permute-start.7
  129.6 1.6 collective-permute-start.14
  131.2 13.8 %collective-permute-done.21 = bf16[1408,256]{1,0:T(8,128)(2,1)S(1)} collective-permute-done((bf16[1408,256]{1,0:T(8,128)(2,1)S(1)}, bf16[1408,256]{1,0:T(8,128)(2,1)S(1)}, u32[]{:S(2)}, u32[]{:S(2)}) %collective-permute-start.21) | collective-permute-done | bytes 720928 | tf_op jit(solution)/shard_map/ppermute | solution.py:78
  152.7 1.6 collective-permute-start.23
  154.3 4.5 %collective-permute-done.6 = bf16[256,1408]{1,0:T(8,128)(2,1)S(1)} collective-permute-done((bf16[256,1408]{1,0:T(8,128)(2,1)}, bf16[256,1408]{1,0:T(8,128)(2,1)S(1)}, u32[]{:S(2)}, u32[]{:S(2)}) %collective-permute-start.6) | collective-permute-done | bytes 720928 | tf_op jit(solution)/shard_map/ppermute | solution.py:77
  158.8 1.6 collective-permute-start.22
  161.2 1.6 collective-permute-start.8
  163.5 10.8 %collective-permute-done.14 = bf16[256,1408]{1,0:T(8,128)(2,1)} collective-permute-done((bf16[256,1408]{1,0:T(8,128)(2,1)}, bf16[256,1408]{1,0:T(8,128)(2,1)}, u32[]{:S(2)}, u32[]{:S(2)}) %collective-permute-start.14) | collective-permute-done | bytes 720928 | tf_op jit(solution)/shard_map/ppermute | solution.py:77
  174.3 1.5 collective-permute-start.9
  175.9 1.8 slice.190
  178.9 2.2 fusion.36
  181.1 1.9 fusion.38
  183.0 3.9 %fusion.40 = f32[768,1408]{1,0:T(8,128)} fusion(bf16[256,1408]{1,0:T(8,128)(2,1)} %collective-permute-done.13, bf16[768,2048]{1,0:T(8,128)(2,1)S(1)} %copy-done, u32[]{:T(128)} %bitcast.16), kind=kOutput, calls=%fused_computation.53 | convolution fusion | flops 553648128 | bytes 5439492 | tf_op jit(solution)/shard_map/dot_general | solution.py:125
  186.9 4.0 %fusion.42 = f32[768,1408]{1,0:T(8,128)} fusion(bf16[256,1408]{1,0:T(8,128)(2,1)} %collective-permute-done.5, bf16[768,2048]{1,0:T(8,128)(2,1)S(1)} %copy-done, u32[]{:T(128)} %bitcast.16), kind=kOutput, calls=%fused_computation.55 | convolution fusion | flops 553648128 | bytes 5439492 | tf_op jit(solution)/shard_map/dot_general | solution.py:125
  190.9 4.0 %fusion.44 = f32[768,1408]{1,0:T(8,128)} fusion(bf16[256,1408]{1,0:T(8,128)(2,1)} %collective-permute-done.12, bf16[768,2048]{1,0:T(8,128)(2,1)S(1)} %copy-done, u32[]{:T(128)} %bitcast.15), kind=kOutput, calls=%fused_computation.57 | convolution fusion | flops 553648128 | bytes 5439492 | tf_op jit(solution)/shard_map/dot_general | solution.py:125
  194.9 4.0 %fusion.46 = f32[768,1408]{1,0:T(8,128)} fusion(bf16[256,1408]{1,0:T(8,128)(2,1)} %collective-permute-done.4, bf16[768,2048]{1,0:T(8,128)(2,1)S(1)} %copy-done, u32[]{:T(128)} %bitcast.15), kind=kOutput, calls=%fused_computation.59 | convolution fusion | flops 553648128 | bytes 5439492 | tf_op jit(solution)/shard_map/dot_general | solution.py:125
  198.9 2.9 fusion.48
  201.7 2.8 fusion.50
  204.6 2.9 fusion.52
  207.5 2.8 fusion.54
  210.3 2.8 fusion.56
  213.0 2.8 fusion.58
  215.8 1.5 collective-permute-start.17
  217.3 4.0 %fusion.17 = f32[768,1408]{1,0:T(8,128)} fusion(bf16[128,1408]{1,0:T(8,128)(2,1)} %collective-permute-done.9, bf16[128,1408]{1,0:T(8,128)(2,1)S(1)} %collective-permute-done.8, bf16[768,2048]{1,0:T(8,128)(2,1)S(1)} %copy-done, u32[]{:T(128)} %bitcast.19), kind=kOutput, calls=%fused_computation.31 | convolution fusion | flops 555089920 | bytes 5439492 | tf_op jit(solution)/shard_map/dot_general | solution.py:125
  221.3 2.8 fusion.32
  224.0 3.8 %fusion.21 = f32[768,1408]{1,0:T(8,128)} fusion(bf16[128,1408]{1,0:T(8,128)(2,1)S(1)} %collective-permute-done.17, bf16[128,1408]{1,0:T(8,128)(2,1)} %collective-permute-done.16, bf16[768,2048]{1,0:T(8,128)(2,1)S(1)} %copy-done, u32[]{:T(128)} %bitcast.19), kind=kOutput, calls=%fused_computation.35 | convolution fusion | flops 555089920 | bytes 5439492 | tf_op jit(solution)/shard_map/dot_general | solution.py:125
  227.8 20.3 %multiply_convert_fusion = bf16[768,1408]{1,0:T(8,128)(2,1)} fusion(f32[768,1408]{1,0:T(8,128)} %fusion.21, f32[768,1408]{1,0:T(8,128)S(1)} %fusion.36, f32[768,1408]{1,0:T(8,128)} %fusion.40, f32[768,1408]{1,0:T(8,128)} %fusion.44, f32[768,1408]{1,0:T(8,128)} %fusion.48, f32[768,1408]{1,0:T(8,128)} %fusion.56, f32[768,1408]{1,0:T(8,128)} %fusion.52, ...), kind=kOutput, calls=%fused_computation | convolution fusion | flops 575275008 | bytes 68157952 | tf_op jit(solution)/shard_map/dot_general | solution.py:125
  248.2 2.7 convolution_convert_fusion.1
  250.9 1.9 convolution_convert_fusion.2
  253.8 1.9 convolution_convert_fusion.3
  255.7 1.9 convolution_convert_fusion.4
  258.7 2.0 convolution_convert_fusion.7
  261.4 1.9 convolution_convert_fusion.6
  269.6 3.5 collective-permute-done.24
  273.0 1.8 collective-permute-done.25
  274.8 1.5 convolution_convert_fusion
  277.3 24.2 %reduce-scatter.7.cloned.1.call-done = bf16[192,512]{1,0:T(8,128)(2,1)} async-done(((bf16[768,512]{1,0:T(8,128)(2,1)}), bf16[192,512]{1,0:T(8,128)(2,1)}) %reduce-scatter.7.cloned.1.call-update) | async-done | bytes 196624 | tf_op jit(solution)/shard_map/reduce_scatter | solution.py:141
  302.5 27.1 %reduce-scatter.5.cloned.1.call-done = bf16[192,768]{1,0:T(8,128)(2,1)} async-done(((bf16[768,768]{1,0:T(8,128)(2,1)}), bf16[192,768]{1,0:T(8,128)(2,1)}) %reduce-scatter.5.cloned.1.call-update) | async-done | bytes 294928 | tf_op jit(solution)/shard_map/reduce_scatter | solution.py:141
  330.6 1.6 fusion.75
  336.2 16.6 %reduce-scatter.11.cloned.1.call-done = bf16[192,256]{1,0:T(8,128)(2,1)} async-done(((bf16[768,256]{1,0:T(8,128)(2,1)}), bf16[192,256]{1,0:T(8,128)(2,1)}) %reduce-scatter.11.cloned.1.call-update) | async-done | bytes 98320 | tf_op jit(solution)/shard_map/reduce_scatter | solution.py:141
  352.8 1.6 fusion.74
  (131 shorter events, 32.9 us)
Async XLA Ops:
  6.5 172.4 %all-gather.2.cloned.1.call-start = ((), (), s32[]{:S(2)}) async-start(), calls=%async_computation.5 | async-start | bytes 3932160 | tf_op jit(solution)/shard_map/all_gather | solution.py:117
  7.3 14.8 %collective-permute-start.1 = (bf16[128,64]{0,1:T(8,128)(2,1)S(1)}, bf16[128,64]{0,1:T(8,128)(2,1)S(1)}, u32[]{:S(2)}, u32[]{:S(2)}) collective-permute-start(bf16[128,64]{0,1:T(8,128)(2,1)S(1)} %slice.149), channel_id=1, source_target_pairs={{0,4},{4,8},{8,12},{12,16},{16,20},{20,24},{24,28},{1,5},{5,9},{9,... | collective-permute-start | bytes 49160 | tf_op jit(solution)/shard_map/ppermute | solution.py:15
  12.9 13.0 %collective-permute-start = (bf16[128,64]{0,1:T(8,128)(2,1)S(1)}, bf16[128,64]{0,1:T(8,128)(2,1)S(1)}, u32[]{:S(2)}, u32[]{:S(2)}) collective-permute-start(bf16[128,64]{0,1:T(8,128)(2,1)S(1)} %slice.147), channel_id=1, source_target_pairs={{0,4},{4,8},{8,12},{12,16},{16,20},{20,24},{24,28},{1,5},{5,9},{9,... | collective-permute-start | bytes 49160 | tf_op jit(solution)/shard_map/ppermute | solution.py:15
  18.8 6.2 %copy-start.21 = (f32[4]{0:T(128)S(1)}, f32[4]{0:T(128)}, u32[]{:S(2)}) copy-start(f32[4]{0:T(128)} %param.17) | copy-start | bytes 52
  23.1 2.8 copy-start.18
  42.1 3.7 %copy-start.20 = (f32[2048]{0:T(1024)S(1)}, f32[2048]{0:T(1024)}, u32[]{:S(2)}) copy-start(f32[2048]{0:T(1024)} %param.19) | copy-start | bytes 24580
  42.1 4.9 %copy-start.8 = (bf16[256,1408]{1,0:T(8,128)(2,1)S(1)}, bf16[256,1408]{1,0:T(8,128)(2,1)}, u32[]{:S(2)}) copy-start(bf16[256,1408]{1,0:T(8,128)(2,1)} %param.20) | copy-start | bytes 2162692
  42.1 7.0 %copy-start.6 = (bf16[256,1408]{1,0:T(8,128)(2,1)S(1)}, bf16[256,1408]{1,0:T(8,128)(2,1)}, u32[]{:S(2)}) copy-start(bf16[256,1408]{1,0:T(8,128)(2,1)} %param.21) | copy-start | bytes 2162692
  47.0 229.4 %reduce-scatter.9.cloned.1.call-start = ((), (), s32[]{:S(2)}) async-start(), calls=%async_computation.8 | async-start | bytes 983040 | tf_op jit(solution)/shard_map/reduce_scatter | solution.py:141
  47.0 19.1 %collective-permute-start.2 = (bf16[256,1408]{1,0:T(8,128)(2,1)S(1)}, bf16[256,1408]{1,0:T(8,128)(2,1)S(1)}, u32[]{:S(2)}, u32[]{:S(2)}) collective-permute-start(bf16[256,1408]{1,0:T(8,128)(2,1)S(1)} %copy-done.8), channel_id=1, source_target_pairs={{0,8},{8,16},{16,24},{24,28},{28,20},{20,12},{12,4},{4,0},{1,9},{9... | collective-permute-start | bytes 2162696 | tf_op jit(solution)/shard_map/ppermute | solution.py:77
  48.7 19.0 %collective-permute-start.3 = (bf16[256,1408]{1,0:T(8,128)(2,1)S(1)}, bf16[256,1408]{1,0:T(8,128)(2,1)S(1)}, u32[]{:S(2)}, u32[]{:S(2)}) collective-permute-start(bf16[256,1408]{1,0:T(8,128)(2,1)S(1)} %copy-done.8), channel_id=1, source_target_pairs={{8,0},{16,8},{24,16},{28,24},{20,28},{12,20},{4,12},{0,4},{9,1},{1... | collective-permute-start | bytes 2162696 | tf_op jit(solution)/shard_map/ppermute | solution.py:78
  49.1 32.4 %collective-permute-start.10 = (bf16[256,1408]{1,0:T(8,128)(2,1)S(1)}, bf16[256,1408]{1,0:T(8,128)(2,1)S(1)}, u32[]{:S(2)}, u32[]{:S(2)}) collective-permute-start(bf16[256,1408]{1,0:T(8,128)(2,1)S(1)} %copy-done.6), channel_id=1, source_target_pairs={{0,8},{8,16},{16,24},{24,28},{28,20},{20,12},{12,4},{4,0},{1,9},{9... | collective-permute-start | bytes 2162696 | tf_op jit(solution)/shard_map/ppermute | solution.py:77
  50.7 32.4 %collective-permute-start.11 = (bf16[256,1408]{1,0:T(8,128)(2,1)S(1)}, bf16[256,1408]{1,0:T(8,128)(2,1)S(1)}, u32[]{:S(2)}, u32[]{:S(2)}) collective-permute-start(bf16[256,1408]{1,0:T(8,128)(2,1)S(1)} %copy-done.6), channel_id=1, source_target_pairs={{8,0},{16,8},{24,16},{28,24},{20,28},{12,20},{4,12},{0,4},{9,1},{1... | collective-permute-start | bytes 2162696 | tf_op jit(solution)/shard_map/ppermute | solution.py:78
  51.1 47.4 %collective-permute-start.19 = (bf16[1408,256]{1,0:T(8,128)(2,1)}, bf16[1408,256]{1,0:T(8,128)(2,1)S(1)}, u32[]{:S(2)}, u32[]{:S(2)}) collective-permute-start(bf16[1408,256]{1,0:T(8,128)(2,1)} %param.22), channel_id=1, source_target_pairs={{8,0},{16,8},{24,16},{28,24},{20,28},{12,20},{4,12},{0,4},{9,1},{1... | collective-permute-start | bytes 2162696 | tf_op jit(solution)/shard_map/ppermute | solution.py:78
  66.1 48.0 %copy-start.10 = (bf16[256,1408]{1,0:T(8,128)(2,1)}, bf16[256,1408]{1,0:T(8,128)(2,1)S(1)}, u32[]{:S(2)}) copy-start(bf16[256,1408]{1,0:T(8,128)(2,1)S(1)} %collective-permute-done.2) | copy-start | bytes 2162692
  66.1 32.9 %collective-permute-start.18 = (bf16[1408,256]{1,0:T(8,128)(2,1)}, bf16[1408,256]{1,0:T(8,128)(2,1)}, u32[]{:S(2)}, u32[]{:S(2)}) collective-permute-start(bf16[1408,256]{1,0:T(8,128)(2,1)} %param.22), channel_id=1, source_target_pairs={{0,8},{8,16},{16,24},{24,28},{28,20},{20,12},{12,4},{4,0},{1,9},{9... | collective-permute-start | bytes 2162696 | tf_op jit(solution)/shard_map/ppermute | solution.py:77
  67.7 63.5 %copy-start.12 = (bf16[256,1408]{1,0:T(8,128)(2,1)}, bf16[256,1408]{1,0:T(8,128)(2,1)S(1)}, u32[]{:S(2)}) copy-start(bf16[256,1408]{1,0:T(8,128)(2,1)S(1)} %collective-permute-done.3) | copy-start | bytes 2162692
  67.7 44.9 %collective-permute-start.4 = (bf16[256,1408]{1,0:T(8,128)(2,1)S(1)}, bf16[256,1408]{1,0:T(8,128)(2,1)}, u32[]{:S(2)}, u32[]{:S(2)}) collective-permute-start(bf16[256,1408]{1,0:T(8,128)(2,1)S(1)} %collective-permute-done.2), channel_id=1, source_target_pairs={{0,8},{8,16},{16,24},{24,28},{28,20},{20,12},{12,4},{4,0},{1,9},{9... | collective-permute-start | bytes 2162696 | tf_op jit(solution)/shard_map/ppermute | solution.py:77
  81.5 63.4 %copy-start.14 = (bf16[256,1408]{1,0:T(8,128)(2,1)}, bf16[256,1408]{1,0:T(8,128)(2,1)S(1)}, u32[]{:S(2)}) copy-start(bf16[256,1408]{1,0:T(8,128)(2,1)S(1)} %collective-permute-done.10) | copy-start | bytes 2162692
  81.5 32.6 %collective-permute-start.5 = (bf16[256,1408]{1,0:T(8,128)(2,1)S(1)}, bf16[256,1408]{1,0:T(8,128)(2,1)}, u32[]{:S(2)}, u32[]{:S(2)}) collective-permute-start(bf16[256,1408]{1,0:T(8,128)(2,1)S(1)} %collective-permute-done.3), channel_id=1, source_target_pairs={{8,0},{16,8},{24,16},{28,24},{20,28},{12,20},{4,12},{0,4},{9,1},{1... | collective-permute-start | bytes 2162696 | tf_op jit(solution)/shard_map/ppermute | solution.py:78
  83.1 61.8 %copy-start.16 = (bf16[256,1408]{1,0:T(8,128)(2,1)}, bf16[256,1408]{1,0:T(8,128)(2,1)S(1)}, u32[]{:S(2)}) copy-start(bf16[256,1408]{1,0:T(8,128)(2,1)S(1)} %collective-permute-done.11) | copy-start | bytes 2162692
  83.1 44.9 %collective-permute-start.12 = (bf16[256,1408]{1,0:T(8,128)(2,1)S(1)}, bf16[256,1408]{1,0:T(8,128)(2,1)}, u32[]{:S(2)}, u32[]{:S(2)}) collective-permute-start(bf16[256,1408]{1,0:T(8,128)(2,1)S(1)} %collective-permute-done.10), channel_id=1, source_target_pairs={{0,8},{8,16},{16,24},{24,28},{28,20},{20,12},{12,4},{4,0},{1,9},{9... | collective-permute-start | bytes 2162696 | tf_op jit(solution)/shard_map/ppermute | solution.py:77
  98.6 46.4 %copy-start.22 = (bf16[1408,256]{1,0:T(8,128)(2,1)}, bf16[1408,256]{1,0:T(8,128)(2,1)S(1)}, u32[]{:S(2)}) copy-start(bf16[1408,256]{1,0:T(8,128)(2,1)S(1)} %collective-permute-done.19) | copy-start | bytes 2162692
  98.6 31.0 %collective-permute-start.13 = (bf16[256,1408]{1,0:T(8,128)(2,1)S(1)}, bf16[256,1408]{1,0:T(8,128)(2,1)}, u32[]{:S(2)}, u32[]{:S(2)}) collective-permute-start(bf16[256,1408]{1,0:T(8,128)(2,1)S(1)} %collective-permute-done.11), channel_id=1, source_target_pairs={{8,0},{16,8},{24,16},{28,24},{20,28},{12,20},{4,12},{0,4},{9,1},{1... | collective-permute-start | bytes 2162696 | tf_op jit(solution)/shard_map/ppermute | solution.py:78
  99.0 45.9 %collective-permute-start.21 = (bf16[1408,256]{1,0:T(8,128)(2,1)S(1)}, bf16[1408,256]{1,0:T(8,128)(2,1)S(1)}, u32[]{:S(2)}, u32[]{:S(2)}) collective-permute-start(bf16[1408,256]{1,0:T(8,128)(2,1)S(1)} %collective-permute-done.19), channel_id=1, source_target_pairs={{8,0},{16,8},{24,16},{28,24},{20,28},{12,20},{4,12},{0,4},{9,1},{1... | collective-permute-start | bytes 2162696 | tf_op jit(solution)/shard_map/ppermute | solution.py:78
  112.5 40.1 %collective-permute-start.20 = (bf16[1408,256]{1,0:T(8,128)(2,1)}, bf16[1408,256]{1,0:T(8,128)(2,1)}, u32[]{:S(2)}, u32[]{:S(2)}) collective-permute-start(bf16[1408,256]{1,0:T(8,128)(2,1)} %collective-permute-done.18), channel_id=1, source_target_pairs={{0,8},{8,16},{16,24},{24,28},{28,20},{20,12},{12,4},{4,0},{1,9},{9... | collective-permute-start | bytes 2162696 | tf_op jit(solution)/shard_map/ppermute | solution.py:77
  114.1 44.6 %collective-permute-start.6 = (bf16[256,1408]{1,0:T(8,128)(2,1)}, bf16[256,1408]{1,0:T(8,128)(2,1)S(1)}, u32[]{:S(2)}, u32[]{:S(2)}) collective-permute-start(bf16[256,1408]{1,0:T(8,128)(2,1)} %collective-permute-done.4), channel_id=1, source_target_pairs={{0,8},{8,16},{16,24},{24,28},{28,20},{20,12},{12,4},{4,0},{1,9},{9... | collective-permute-start | bytes 2162696 | tf_op jit(solution)/shard_map/ppermute | solution.py:77
  128.0 33.2 %collective-permute-start.7 = (bf16[256,1408]{1,0:T(8,128)(2,1)}, bf16[256,1408]{1,0:T(8,128)(2,1)S(1)}, u32[]{:S(2)}, u32[]{:S(2)}) collective-permute-start(bf16[256,1408]{1,0:T(8,128)(2,1)} %collective-permute-done.5), channel_id=1, source_target_pairs={{8,0},{16,8},{24,16},{28,24},{20,28},{12,20},{4,12},{0,4},{9,1},{1... | collective-permute-start | bytes 2162696 | tf_op jit(solution)/shard_map/ppermute | solution.py:78
  129.6 44.8 %collective-permute-start.14 = (bf16[256,1408]{1,0:T(8,128)(2,1)}, bf16[256,1408]{1,0:T(8,128)(2,1)}, u32[]{:S(2)}, u32[]{:S(2)}) collective-permute-start(bf16[256,1408]{1,0:T(8,128)(2,1)} %collective-permute-done.12), channel_id=1, source_target_pairs={{0,8},{8,16},{16,24},{24,28},{28,20},{20,12},{12,4},{4,0},{1,9},{9... | collective-permute-start | bytes 2162696 | tf_op jit(solution)/shard_map/ppermute | solution.py:77
  144.9 0.9 copy-start.24
  145.8 31.8 %collective-permute-start.15 = (bf16[256,1408]{1,0:T(8,128)(2,1)}, bf16[256,1408]{1,0:T(8,128)(2,1)S(1)}, u32[]{:S(2)}, u32[]{:S(2)}) collective-permute-start(bf16[256,1408]{1,0:T(8,128)(2,1)} %collective-permute-done.13), channel_id=1, source_target_pairs={{8,0},{16,8},{24,16},{28,24},{20,28},{12,20},{4,12},{0,4},{9,1},{1... | collective-permute-start | bytes 2162696 | tf_op jit(solution)/shard_map/ppermute | solution.py:78
  152.7 95.5 %collective-permute-start.23 = (bf16[1408,256]{1,0:T(8,128)(2,1)}, bf16[1408,256]{1,0:T(8,128)(2,1)}, u32[]{:S(2)}, u32[]{:S(2)}) collective-permute-start(bf16[1408,256]{1,0:T(8,128)(2,1)} %copy-done.24), channel_id=1, source_target_pairs={{8,0},{16,8},{24,16},{28,24},{20,28},{12,20},{4,12},{0,4},{9,1},{1... | collective-permute-start | bytes 2162696 | tf_op jit(solution)/shard_map/ppermute | solution.py:78
  158.8 20.1 %copy-start.5 = (bf16[256,1408]{1,0:T(8,128)(2,1)}, bf16[256,1408]{1,0:T(8,128)(2,1)S(1)}, u32[]{:S(2)}) copy-start(bf16[256,1408]{1,0:T(8,128)(2,1)S(1)} %collective-permute-done.6) | copy-start | bytes 2162692
  158.8 92.1 %collective-permute-start.22 = (bf16[1408,256]{1,0:T(8,128)(2,1)}, bf16[1408,256]{1,0:T(8,128)(2,1)}, u32[]{:S(2)}, u32[]{:S(2)}) collective-permute-start(bf16[1408,256]{1,0:T(8,128)(2,1)} %collective-permute-done.20), channel_id=1, source_target_pairs={{0,8},{8,16},{16,24},{24,28},{28,20},{20,12},{12,4},{4,0},{1,9},{9... | collective-permute-start | bytes 2162696 | tf_op jit(solution)/shard_map/ppermute | solution.py:77
  161.2 17.7 %copy-start.3 = (bf16[256,1408]{1,0:T(8,128)(2,1)}, bf16[256,1408]{1,0:T(8,128)(2,1)S(1)}, u32[]{:S(2)}) copy-start(bf16[256,1408]{1,0:T(8,128)(2,1)S(1)} %collective-permute-done.7) | copy-start | bytes 2162692
  161.2 54.7 %collective-permute-start.8 = (bf16[128,1408]{1,0:T(8,128)(2,1)}, bf16[128,1408]{1,0:T(8,128)(2,1)S(1)}, u32[]{:S(2)}, u32[]{:S(2)}) collective-permute-start(bf16[128,1408]{1,0:T(8,128)(2,1)} %slice.188), channel_id=1, source_target_pairs={{0,8},{8,16},{16,24},{24,28},{28,20},{20,12},{12,4},{4,0},{1,9},{9... | collective-permute-start | bytes 1081352 | tf_op jit(solution)/shard_map/ppermute | solution.py:81
  174.3 43.0 %collective-permute-start.9 = (bf16[128,1408]{1,0:T(8,128)(2,1)}, bf16[128,1408]{1,0:T(8,128)(2,1)}, u32[]{:S(2)}, u32[]{:S(2)}) collective-permute-start(bf16[128,1408]{1,0:T(8,128)(2,1)} %slice.189), channel_id=1, source_target_pairs={{8,0},{16,8},{24,16},{28,24},{20,28},{12,20},{4,12},{0,4},{9,1},{1... | collective-permute-start | bytes 1081352 | tf_op jit(solution)/shard_map/ppermute | solution.py:82
  177.6 1.3 copy-start.2
  177.6 46.4 %collective-permute-start.16 = (bf16[128,1408]{1,0:T(8,128)(2,1)}, bf16[128,1408]{1,0:T(8,128)(2,1)}, u32[]{:S(2)}, u32[]{:S(2)}) collective-permute-start(bf16[128,1408]{1,0:T(8,128)(2,1)} %slice.190), channel_id=1, source_target_pairs={{0,8},{8,16},{16,24},{24,28},{28,20},{20,12},{12,4},{4,0},{1,9},{9... | collective-permute-start | bytes 1081352 | tf_op jit(solution)/shard_map/ppermute | solution.py:81
  178.9 2.2 copy-start
  194.9 4.0 %copy-start.17 = (bf16[256,1408]{1,0:T(8,128)(2,1)S(1)}, bf16[256,1408]{1,0:T(8,128)(2,1)}, u32[]{:S(2)}) copy-start(bf16[256,1408]{1,0:T(8,128)(2,1)} %copy-done.16) | copy-start | bytes 2162692
  198.9 2.9 copy-start.13
  201.7 2.8 copy-start.15
  204.6 2.9 copy-start.11
  207.5 2.8 copy-start.7
  210.3 2.8 copy-start.9
  213.0 2.8 copy-start.19
  215.8 8.2 %collective-permute-start.17 = (bf16[128,1408]{1,0:T(8,128)(2,1)S(1)}, bf16[128,1408]{1,0:T(8,128)(2,1)S(1)}, u32[]{:S(2)}, u32[]{:S(2)}) collective-permute-start(bf16[128,1408]{1,0:T(8,128)(2,1)S(1)} %copy-done.19), channel_id=1, source_target_pairs={{8,0},{16,8},{24,16},{28,24},{20,28},{12,20},{4,12},{0,4},{9,1},{1... | collective-permute-start | bytes 1081352 | tf_op jit(solution)/shard_map/ppermute | solution.py:82
  217.3 4.0 %copy-start.4 = (bf16[256,1408]{1,0:T(8,128)(2,1)S(1)}, bf16[256,1408]{1,0:T(8,128)(2,1)}, u32[]{:S(2)}) copy-start(bf16[256,1408]{1,0:T(8,128)(2,1)} %copy-done.3) | copy-start | bytes 2162692
  248.2 2.7 copy-start.1
  253.8 47.8 %reduce-scatter.7.cloned.1.call-start = ((), (), s32[]{:S(2)}) async-start(), calls=%async_computation.7 | async-start | bytes 983040 | tf_op jit(solution)/shard_map/reduce_scatter | solution.py:141
  258.6 71.0 %reduce-scatter.5.cloned.1.call-start = ((), (), s32[]{:S(2)}) async-start(), calls=%async_computation.6 | async-start | bytes 1474560 | tf_op jit(solution)/shard_map/reduce_scatter | solution.py:141
  258.6 2.0 copy-start.23
  264.5 88.3 %reduce-scatter.11.cloned.1.call-start = ((), (), s32[]{:S(2)}) async-start(), calls=%async_computation.9 | async-start | bytes 491520 | tf_op jit(solution)/shard_map/reduce_scatter | solution.py:141
  265.5 7.5 %collective-permute-start.24 = (bf16[704,256]{1,0:T(8,128)(2,1)S(1)}, bf16[704,256]{1,0:T(8,128)(2,1)S(1)}, u32[]{:S(2)}, u32[]{:S(2)}) collective-permute-start(bf16[704,256]{1,0:T(8,128)(2,1)S(1)} %slice.199), channel_id=1, source_target_pairs={{0,8},{8,16},{16,24},{24,28},{28,20},{20,12},{12,4},{4,0},{1,9},{9... | collective-permute-start | bytes 1081352 | tf_op jit(solution)/shard_map/ppermute | solution.py:81
  267.3 7.5 %collective-permute-start.25 = (bf16[704,256]{1,0:T(8,128)(2,1)S(1)}, bf16[704,256]{1,0:T(8,128)(2,1)S(1)}, u32[]{:S(2)}, u32[]{:S(2)}) collective-permute-start(bf16[704,256]{1,0:T(8,128)(2,1)S(1)} %slice.200), channel_id=1, source_target_pairs={{8,0},{16,8},{24,16},{28,24},{20,28},{12,20},{4,12},{0,4},{9,1},{1... | collective-permute-start | bytes 1081352 | tf_op jit(solution)/shard_map/ppermute | solution.py:82
Sparse Core Ops, SparseCore 0:
  47.1 27.8 all-gather.1
  253.9 21.8 reduce-scatter.8
  278.3 23.1 reduce-scatter.6
  304.0 25.6 reduce-scatter.4
  332.0 20.7 reduce-scatter.10

commit v2 on v1

--- a/solution.py
+++ b/solution.py
@@ -1,6 +1,8 @@
 import jax
 import jax.numpy as jnp
 from jax import lax
+from jax.experimental import pallas as pl
+from jax.experimental.pallas import tpu as pltpu
 from jax.sharding import PartitionSpec as P
 
 
@@ -51,6 +53,73 @@
     return list(range(0, count, 2)) + list(range(1, count, 2))[::-1]
 
 
+def widen_body(starts, normed, *refs):
+    count = (len(refs) - 2) // 2
+    gates, ups = refs[:count], refs[count : 2 * count]
+    hidden, ordered = refs[-2:]
+    base = 0
+    for at, ref in enumerate(gates):
+        depth = ref.shape[0]
+        first = pl.multiple_of(starts[at], LANES)
+        ordered[:, base : base + depth] = normed[:, pl.ds(first, depth)]
+        base += depth
+    total = hidden.shape[1]
+    rows = ordered[...]
+    for low in range(0, total, 2 * LANES):
+        high = min(low + 2 * LANES, total)
+        gate = jnp.dot(
+            rows,
+            jnp.concatenate([ref[:, low:high] for ref in gates], axis=0),
+            preferred_element_type=jnp.float32,
+        )
+        upper = jnp.dot(
+            rows,
+            jnp.concatenate([ref[:, low:high] for ref in ups], axis=0),
+            preferred_element_type=jnp.float32,
+        )
+        hidden[:, low:high] = (gate / (1.0 + jnp.exp(-gate)) * upper).astype(jnp.bfloat16)
+
+
+def widened(normed, gates, ups, starts):
+    rows, depth = normed.shape
+    total = gates[0].shape[1]
+    tile = 256 if rows % 256 == 0 else rows
+    fixed = [pl.BlockSpec(block.shape, lambda i, s: (0, 0)) for block in gates + ups]
+    return pl.pallas_call(
+        widen_body,
+        grid_spec=pltpu.PrefetchScalarGridSpec(
+            num_scalar_prefetch=1,
+            grid=(rows // tile,),
+            in_specs=[pl.BlockSpec((tile, depth), lambda i, s: (i, 0))] + fixed,
+            out_specs=pl.BlockSpec((tile, total), lambda i, s: (i, 0)),
+            scratch_shapes=[pltpu.VMEM((tile, depth), jnp.bfloat16)],
+        ),
+        out_shape=jax.ShapeDtypeStruct((rows, total), jnp.bfloat16),
+        compiler_params=pltpu.CompilerParams(
+            dimension_semantics=("arbitrary",), vmem_limit_bytes=48 * 1024 * 1024
+        ),
+        cost_estimate=pl.CostEstimate(
+            flops=4 * rows * depth * total,
+            transcendentals=rows * total,
+            bytes_accessed=4 * depth * total + 2 * rows * (depth + total),
+        ),
+    )(starts, normed, *gates, *ups)
+
+
+def exchanged(blocks):
+    count = lax.axis_size("tp")
+    me = lax.axis_index("tp").astype(jnp.uint32)
+    size = blocks.shape[0] // count
+    pairs = []
+    for step in range(count):
+        there = (me + step) % count
+        block = lax.dynamic_slice_in_dim(blocks, there * size, size, 0)
+        if step:
+            block = lax.ppermute(block, "tp", [(i, (i + step) % count) for i in range(count)])
+        pairs.append(((me + count - step) % count, block))
+    return pairs
+
+
 def uses_ring(count, widths):
     return count > 1 and count % 2 == 0 and min(widths) >= LANES
 
@@ -58,7 +127,7 @@
 def ring_hops(shard, axis, dim):
     count = lax.axis_size(axis)
     if not uses_ring(count, (shard.shape[dim],)):
-        return [[(jnp.uint32(0), lax.all_gather(shard, axis, axis=dim, tiled=True))]]
+        return [[(jnp.uint32(0), 0, lax.all_gather(shard, axis, axis=dim, tiled=True))]]
     order = ring_order(count)
     place = [0] * count
     for at, dev in enumerate(order):
@@ -71,16 +140,16 @@
     def owner(step):
         return owners[step % count]
 
-    hops = [[(owner(0), shard)]]
+    hops = [[(owner(0), 0, shard)]]
     from_left = from_right = shard
     for step in range(1, count // 2):
         from_left = lax.ppermute(from_left, axis, ahead)
         from_right = lax.ppermute(from_right, axis, back)
-        hops.append([(owner(-step), from_left), (owner(step), from_right)])
+        hops.append([(owner(-step), 0, from_left), (owner(step), 0, from_right)])
     half = shard.shape[0] // 2
     top = lax.ppermute(from_left[:half], axis, ahead)
     bottom = lax.ppermute(from_right[half:], axis, back)
-    hops.append([(owner(count // 2), jnp.concatenate([top, bottom], axis=0))])
+    hops.append([(owner(count // 2), 0, top), (owner(count // 2), half, bottom)])
     return hops
 
 
@@ -107,8 +176,12 @@
     attention = attend(
         queries, keys_ext, values_ext, sinks, lax.axis_index("sp") * (rows_dev // WINDOW)
     )
-    attention = lax.all_to_all(attention, "tp", split_axis=0, concat_axis=1, tiled=True)
-    proj = jnp.dot(attention, out_weight, preferred_element_type=jnp.float32)
+    swapped = exchanged(attention)
+    width = attention.shape[1]
+    heads = jnp.zeros((residual.shape[0], out_weight.shape[0]), jnp.bfloat16)
+    for source, block in swapped:
+        heads = lax.dynamic_update_slice_in_dim(heads, block, source * width, 1)
+    proj = jnp.dot(heads, out_weight, preferred_element_type=jnp.float32)
     mixed = (residual.astype(jnp.float32) + proj).astype(jnp.bfloat16)
     mixf = mixed.astype(jnp.float32)
     normed = (
@@ -116,29 +189,27 @@
     ).astype(jnp.bfloat16)
     normed_all = lax.all_gather(normed, "tp", axis=0, tiled=True)
 
-    def contracted(hops):
-        total = None
-        for hop in hops:
-            for owner, block in hop:
-                depth = block.shape[0]
-                rows = lax.dynamic_slice_in_dim(normed_all, owner * depth, depth, 1)
-                part = jnp.dot(rows, block, preferred_element_type=jnp.float32)
-                total = part if total is None else total + part
-        return total
-
-    gate = contracted(gate_hops)
-    upper = contracted(up_hops)
-    hidden = (jax.nn.silu(gate) * upper).astype(jnp.bfloat16)
-    groups = down_hops[1:]
-    groups = [down_hops[0] + groups[0]] + groups[1:] if groups else down_hops
+    depth = gate_hops[0][0][2].shape[0]
+    pieces = [piece for hop in gate_hops for piece in hop]
+    starts = jnp.stack([owner.astype(jnp.int32) * depth + at for owner, at, _ in pieces])
+    gates = [block for _, _, block in pieces]
+    ups = [block for hop in up_hops for _, _, block in hop]
+    hidden = widened(normed_all, gates, ups, starts)
+
+    merged = [[(owner, block) for owner, _, block in hop] for hop in down_hops]
+    if len(merged) > 1:
+        merged[-1] = [
+            (merged[-1][0][0], jnp.concatenate([block for _, block in merged[-1]], axis=0))
+        ]
+        merged = [merged[0] + merged[1]] + merged[2:]
     out = mixed
-    for group in groups:
+    for group in merged:
         parts = [
             jnp.dot(hidden, block, preferred_element_type=jnp.float32).astype(jnp.bfloat16)
             for _, block in group
         ]
         terms = jnp.concatenate(parts, axis=1)
-        ffn = lax.psum_scatter(terms, "tp", scatter_dimension=0, tiled=True).astype(jnp.float32)
+        ffn = sum(block.astype(jnp.float32) for _, block in exchanged(terms))
         for at, (owner, block) in enumerate(group):
             width = block.shape[1]
             base = lax.dynamic_slice_in_dim(mixed, owner * width, width, 1).astype(jnp.float32)

time: 362 us -> 274 us (0.76)
  matrix products: 90.3 us -> 19.4 us
  waiting for transfers between devices: 166 us -> 135 us
  Pallas kernels: 0 us -> 15.1 us
  other arithmetic: 17 us -> 4.54 us
  starting transfers between devices: 39.5 us -> 50.4 us
  blocking collectives: 9.97 us -> 0 us
  between operations: 18.6 us -> 24 us
  local copies, waits for them, and re-layouts: 19.2 us -> 24.5 us
    dot_general x17 -> x1, matrix products: 71.3 us -> 3.34 us  [shards(): proj = jnp.dot(heads, out_weight, preferred_element_type=jnp.float32)]
    reduce_scatter x4 -> x0, waiting for transfers between devices: 68 us -> none  [shards(): lax.psum_scatter(terms, 'tp', scatter_dimension=0, tiled=True)]
    ppermute x0 -> x15, waiting for transfers between devices: none -> 22.9 us  [exchanged(): lax.ppermute(block, 'tp', [(i, (i + step) % count) for i in range(count)])]
    ppermute x9, waiting for transfers between devices: 65.3 us -> 83.7 us  [ring_hops(): from_left = lax.ppermute(from_left, axis, ahead)]
    pallas_call x0 -> x1, Pallas kernels: none -> 15.1 us  [widened(): pl.pallas_call(widen_body, grid_spec=pltpu.PrefetchScalarGridSpec(num_sca...]
    ppermute x0 -> x15, starting transfers between devices: none -> 12.3 us  [exchanged(): lax.ppermute(block, 'tp', [(i, (i + step) % count) for i in range(count)])]
    all_to_all x1 -> x0, blocking collectives: 9.97 us -> none  [shards(): lax.all_to_all(attention, 'tp', split_axis=0, concat_axis=1, tiled=True)]
    dynamic_update_slice x8, other arithmetic: 7.13 us -> 0.96 us  [shards(): out = lax.dynamic_update_slice_in_dim(out, piece, owner * width, 1)]
  transfers between devices with their start and end apart: 31 -> 42, of which waited for: 15 -> 19; matrix products, arithmetic and copies ran while one was open for 30% -> 12% of each run, Pallas kernels for 0% -> 6%
where the time goes in v2:
time: 274 us; the launch traced here: 272 us
  waiting for transfers between devices  135 us (49%)
  starting transfers between devices  50.4 us (18%)
  local copies, waits for them, and re-layouts  24.5 us (9%)
  between operations  24 us (9%)
  matrix products  19.4 us (7%)
  Pallas kernels  15.1 us (6%)
  other arithmetic  4.54 us (2%)
    ppermute x9, waiting for transfers between devices, ring_hops(): from_left = lax.ppermute(from_left, axis, ahead)  83.7 us
    ppermute x9, waiting for transfers between devices, ring_hops(): from_right = lax.ppermute(from_right, axis, back)  27.9 us
    ppermute x15, waiting for transfers between devices, exchanged(): lax.ppermute(block, 'tp', [(i, (i + step) % count) for i in range(count)])  22.9 us
    pallas_call x1, Pallas kernels, widened(): pl.pallas_call(widen_body, grid_spec=pltpu.PrefetchScalarGridSpec(num_sca...  15.1 us
    ppermute x9, starting transfers between devices, ring_hops(): from_left = lax.ppermute(from_left, axis, ahead)  13.4 us
    dot_general x8, matrix products, shards(): jnp.dot(hidden, block, preferred_element_type=jnp.float32)  12.4 us
    ppermute x15, starting transfers between devices, exchanged(): lax.ppermute(block, 'tp', [(i, (i + step) % count) for i in range(count)])  12.3 us
    ppermute x9, starting transfers between devices, ring_hops(): from_right = lax.ppermute(from_right, axis, back)  9.49 us
  transfers between devices with their start and end apart: 42, of which 19 were waited for; matrix products, arithmetic and copies ran while one was open for 12% of the time, Pallas kernels for 6%

profile of v2, /device:TPU:0, one launch (start us, length us, event | category | flops | bytes accessed | tf_op | source)
XLA Modules:
  0.0 272.4 jit_solution(8960606345704973820)
XLA Ops:
  7.3 4.9 %collective-permute-start.1 = (bf16[128,64]{0,1:T(8,128)(2,1)S(1)}, bf16[128,64]{0,1:T(8,128)(2,1)S(1)}, u32[]{:S(2)}, u32[]{:S(2)}) collective-permute-start(bf16[128,64]{0,1:T(8,128)(2,1)S(1)} %slice.118), channel_id=1, source_target_pairs={{0,4},{4,8},{8,12},{12,16},{16,20},{20,24},{24,28},{1,5},{5,9},{9,... | collective-permute-start | bytes 49160 | tf_op jit(solution)/shard_map/ppermute | solution.py:17
  12.9 3.4 %collective-permute-start = (bf16[128,64]{0,1:T(8,128)(2,1)S(1)}, bf16[128,64]{0,1:T(8,128)(2,1)S(1)}, u32[]{:S(2)}, u32[]{:S(2)}) collective-permute-start(bf16[128,64]{0,1:T(8,128)(2,1)S(1)} %slice.116), channel_id=1, source_target_pairs={{0,4},{4,8},{8,12},{12,16},{16,20},{20,24},{24,28},{1,5},{5,9},{9,... | collective-permute-start | bytes 49160 | tf_op jit(solution)/shard_map/ppermute | solution.py:17
  16.8 1.0 reshape.228
  17.8 1.0 reshape.225
  18.9 2.5 reshape.234
  22.3 1.9 fusion.2
  25.7 1.0 reshape.224
  26.7 1.8 fusion.12
  29.3 1.5 collective-permute-start.3
  30.8 1.4 collective-permute-start.4
  32.2 2.2 collective-permute-done.2
  34.4 1.3 collective-permute-done.3
  35.7 1.1 collective-permute-done.4
  36.9 3.3 %fusion.3 = (f32[192]{0:T(256)S(1)}, bf16[192,2048]{1,0:T(8,128)(2,1)S(1)}) fusion(bf16[192,1024]{0,1:T(8,128)(2,1)S(1)} %constant_dynamic-update-slice_fusion, bf16[1024,2048]{1,0:T(8,128)(2,1)} %param.17, bf16[192,2048]{1,0:T(8,128)(2,1)S(1)} %copy-done.16), kind=kOutput, calls=%fused_computation.9 | convolution fusion | flops 807665472 | bytes 6161152 | tf_op jit(solution)/shard_map/dot_general | solution.py:184
  41.2 1.1 fusion.5
  42.3 1.6 collective-permute-start.5
  44.4 1.6 collective-permute-start.13
  46.4 1.5 collective-permute-start.22
  48.0 13.4 %collective-permute-done.5.refs_1_ = bf16[256,1408]{1,0:T(8,128)(2,1)S(1)} collective-permute-done((bf16[256,1408]{1,0:T(8,128)(2,1)S(1)}, bf16[256,1408]{1,0:T(8,128)(2,1)S(1)}, u32[]{:S(2)}, u32[]{:S(2)}) %collective-permute-start.5) | collective-permute-done | bytes 720928 | tf_op jit(solution)/shard_map/ppermute | solution.py:146
  61.4 1.6 collective-permute-start.21
  63.0 1.6 collective-permute-start.7
  64.5 12.3 %collective-permute-done.13.refs_10_ = bf16[256,1408]{1,0:T(8,128)(2,1)S(1)} collective-permute-done((bf16[256,1408]{1,0:T(8,128)(2,1)S(1)}, bf16[256,1408]{1,0:T(8,128)(2,1)S(1)}, u32[]{:S(2)}, u32[]{:S(2)}) %collective-permute-start.13) | collective-permute-done | bytes 720928 | tf_op jit(solution)/shard_map/ppermute | solution.py:146
  76.8 1.5 collective-permute-start.8
  78.4 1.6 collective-permute-start.15
  80.0 13.9 %collective-permute-done.22 = bf16[1408,256]{1,0:T(8,128)(2,1)S(1)} collective-permute-done((bf16[1408,256]{1,0:T(8,128)(2,1)}, bf16[1408,256]{1,0:T(8,128)(2,1)S(1)}, u32[]{:S(2)}, u32[]{:S(2)}) %collective-permute-start.22) | collective-permute-done | bytes 720928 | tf_op jit(solution)/shard_map/ppermute | solution.py:147
  94.3 1.5 collective-permute-start.27
  95.9 11.9 %collective-permute-done.7.refs_3_ = bf16[256,1408]{1,0:T(8,128)(2,1)S(1)} collective-permute-done((bf16[256,1408]{1,0:T(8,128)(2,1)S(1)}, bf16[256,1408]{1,0:T(8,128)(2,1)S(1)}, u32[]{:S(2)}, u32[]{:S(2)}) %collective-permute-start.7) | collective-permute-done | bytes 720928 | tf_op jit(solution)/shard_map/ppermute | solution.py:146
  107.7 1.6 collective-permute-start.26
  109.3 1.6 collective-permute-start.9
  111.8 11.4 %collective-permute-done.15.refs_12_ = bf16[256,1408]{1,0:T(8,128)(2,1)S(1)} collective-permute-done((bf16[256,1408]{1,0:T(8,128)(2,1)S(1)}, bf16[256,1408]{1,0:T(8,128)(2,1)S(1)}, u32[]{:S(2)}, u32[]{:S(2)}) %collective-permute-start.15) | collective-permute-done | bytes 720928 | tf_op jit(solution)/shard_map/ppermute | solution.py:146
  123.2 1.5 collective-permute-start.10
  126.3 14.0 %collective-permute-done.27 = bf16[1408,256]{1,0:T(8,128)(2,1)} collective-permute-done((bf16[1408,256]{1,0:T(8,128)(2,1)S(1)}, bf16[1408,256]{1,0:T(8,128)(2,1)}, u32[]{:S(2)}, u32[]{:S(2)}) %collective-permute-start.27) | collective-permute-done | bytes 720928 | tf_op jit(solution)/shard_map/ppermute | solution.py:147
  140.8 1.6 collective-permute-start.31
  142.3 11.7 %collective-permute-done.9.refs_5_ = bf16[256,1408]{1,0:T(8,128)(2,1)S(1)} collective-permute-done((bf16[256,1408]{1,0:T(8,128)(2,1)S(1)}, bf16[256,1408]{1,0:T(8,128)(2,1)S(1)}, u32[]{:S(2)}, u32[]{:S(2)}) %collective-permute-start.9) | collective-permute-done | bytes 720928 | tf_op jit(solution)/shard_map/ppermute | solution.py:146
  154.1 1.6 collective-permute-start.32
  158.1 11.4 %collective-permute-done.17.refs_14_ = bf16[256,1408]{1,0:T(8,128)(2,1)S(1)} collective-permute-done((bf16[256,1408]{1,0:T(8,128)(2,1)S(1)}, bf16[256,1408]{1,0:T(8,128)(2,1)S(1)}, u32[]{:S(2)}, u32[]{:S(2)}) %collective-permute-start.17) | collective-permute-done | bytes 720928 | tf_op jit(solution)/shard_map/ppermute | solution.py:146
  169.5 1.5 collective-permute-start.12
  171.9 0.9 collective-permute-start.19
  173.6 11.5 %collective-permute-done.31 = bf16[1408,256]{1,0:T(8,128)(2,1)} collective-permute-done((bf16[1408,256]{1,0:T(8,128)(2,1)S(1)}, bf16[1408,256]{1,0:T(8,128)(2,1)}, u32[]{:S(2)}, u32[]{:S(2)}) %collective-permute-start.31) | collective-permute-done | bytes 720928 | tf_op jit(solution)/shard_map/ppermute | solution.py:146
  185.1 1.5 collective-permute-start.20
  198.1 2.1 copy.60
  200.2 1.7 slice.160
  202.4 1.8 slice.161
  204.2 1.5 collective-permute-start.37
  205.8 1.1 copy-done.2
  206.9 1.1 copy-done.4
  208.0 15.1 %shard_map.118 = bf16[768,1408]{1,0:T(8,128)(2,1)} custom-call(s32[9]{0:T(128)S(1)} %stack.39.starts, bf16[768,2048]{1,0:T(8,128)(2,1)} %all-gather.2.cloned.1.call-done.normed, bf16[256,1408]{1,0:T(8,128)(2,1)S(1)} %copy-done, bf16[256,1408]{1,0:T(8,128)(2,1)S(1)} %collective-permute-done.5.refs_1_, bf16[256,1408]{1,0:T(8,128)(2,1)S(1)} %collective-permute-done.6.refs_2_, ...), custom_call_target="tpu_custom_call" | custom-call | flops 8858370048 | bytes 16842752 | tf_op jit(solution)/shard_map/pallas_call | solution.py:88
  223.1 2.5 convolution_convert_fusion.7
  225.7 1.9 convolution_convert_fusion.1
  227.6 1.9 convolution_convert_fusion.2
  230.2 1.1 collective-permute-start.35
  231.3 1.9 convolution_convert_fusion.3
  236.6 1.6 collective-permute-start.29
  238.2 1.9 convolution_convert_fusion
  240.2 1.4 collective-permute-start.30
  242.1 2.4 collective-permute-done.28
  244.7 1.2 collective-permute-done.29
  245.8 2.7 collective-permute-start.38
  248.6 1.0 collective-permute-start.39
  249.7 5.4 %collective-permute-done.23 = bf16[192,768]{1,0:T(8,128)(2,1)S(1)} collective-permute-done((bf16[192,768]{1,0:T(8,128)(2,1)S(1)}, bf16[192,768]{1,0:T(8,128)(2,1)S(1)}, u32[]{:S(2)}, u32[]{:S(2)}) %collective-permute-start.23) | collective-permute-done | bytes 294944 | tf_op jit(solution)/shard_map/ppermute | solution.py:118
  255.1 1.3 collective-permute-done.24
  256.4 4.0 %collective-permute-done.25 = bf16[192,768]{1,0:T(8,128)(2,1)S(1)} collective-permute-done((bf16[192,768]{1,0:T(8,128)(2,1)S(1)}, bf16[192,768]{1,0:T(8,128)(2,1)S(1)}, u32[]{:S(2)}, u32[]{:S(2)}) %collective-permute-start.25) | collective-permute-done | bytes 294944 | tf_op jit(solution)/shard_map/ppermute | solution.py:118
  260.8 2.7 collective-permute-done.38
  263.5 1.3 collective-permute-done.39
  (150 shorter events, 22.1 us)
Async XLA Ops:
  6.5 15.6 %copy-start.9 = (bf16[768,64]{0,1:T(8,128)(2,1)S(1)}, bf16[768,64]{0,1:T(8,128)(2,1)}, u32[]{:S(2)}) copy-start(bf16[768,64]{0,1:T(8,128)(2,1)} %param.14) | copy-start | bytes 294916
  6.5 199.2 %all-gather.2.cloned.1.call-start = ((), (), s32[]{:S(2)}) async-start(), calls=%async_computation | async-start | bytes 3932160 | tf_op jit(solution)/shard_map/all_gather | solution.py:190
  7.3 14.8 %collective-permute-start.1 = (bf16[128,64]{0,1:T(8,128)(2,1)S(1)}, bf16[128,64]{0,1:T(8,128)(2,1)S(1)}, u32[]{:S(2)}, u32[]{:S(2)}) collective-permute-start(bf16[128,64]{0,1:T(8,128)(2,1)S(1)} %slice.118), channel_id=1, source_target_pairs={{0,4},{4,8},{8,12},{12,16},{16,20},{20,24},{24,28},{1,5},{5,9},{9,... | collective-permute-start | bytes 49160 | tf_op jit(solution)/shard_map/ppermute | solution.py:17
  12.9 12.1 %collective-permute-start = (bf16[128,64]{0,1:T(8,128)(2,1)S(1)}, bf16[128,64]{0,1:T(8,128)(2,1)S(1)}, u32[]{:S(2)}, u32[]{:S(2)}) collective-permute-start(bf16[128,64]{0,1:T(8,128)(2,1)S(1)} %slice.116), channel_id=1, source_target_pairs={{0,4},{4,8},{8,12},{12,16},{16,20},{20,24},{24,28},{1,5},{5,9},{9,... | collective-permute-start | bytes 49160 | tf_op jit(solution)/shard_map/ppermute | solution.py:17
  22.3 1.9 copy-start.15
  28.6 8.3 %copy-start.16 = (bf16[192,2048]{1,0:T(8,128)(2,1)S(1)}, bf16[192,2048]{1,0:T(8,128)(2,1)}, u32[]{:S(2)}) copy-start(bf16[192,2048]{1,0:T(8,128)(2,1)} %param.12) | copy-start | bytes 2359300
  29.2 5.2 %collective-permute-start.2 = (bf16[192,256]{0,1:T(8,128)(2,1)S(1)}, bf16[192,256]{0,1:T(8,128)(2,1)S(1)}, u32[]{:S(2)}, u32[]{:S(2)}) collective-permute-start(bf16[192,256]{0,1:T(8,128)(2,1)S(1)} %get-tuple-element.19), channel_id=1, source_target_pairs={{0,1},{1,2},{2,3},{3,0},{4,5},{5,6},{6,7},{7,4},{8,9},{9,10},{10,1... | collective-permute-start | bytes 294920 | tf_op jit(solution)/shard_map/ppermute | solution.py:118
  29.3 6.4 %collective-permute-start.3 = (bf16[192,256]{0,1:T(8,128)(2,1)S(1)}, bf16[192,256]{0,1:T(8,128)(2,1)S(1)}, u32[]{:S(2)}, u32[]{:S(2)}) collective-permute-start(bf16[192,256]{0,1:T(8,128)(2,1)S(1)} %get-tuple-element.18), channel_id=1, source_target_pairs={{0,2},{1,3},{2,0},{3,1},{4,6},{5,7},{6,4},{7,5},{8,10},{9,11},{10,... | collective-permute-start | bytes 294920 | tf_op jit(solution)/shard_map/ppermute | solution.py:118
  30.8 6.0 %collective-permute-start.4 = (bf16[192,256]{0,1:T(8,128)(2,1)S(1)}, bf16[192,256]{0,1:T(8,128)(2,1)S(1)}, u32[]{:S(2)}, u32[]{:S(2)}) collective-permute-start(bf16[192,256]{0,1:T(8,128)(2,1)S(1)} %get-tuple-element.17), channel_id=1, source_target_pairs={{0,3},{1,0},{2,1},{3,2},{4,7},{5,4},{6,5},{7,6},{8,11},{9,8},{10,9... | collective-permute-start | bytes 294920 | tf_op jit(solution)/shard_map/ppermute | solution.py:118
  36.9 4.2 %copy-start.14 = (f32[2048]{0:T(1024)S(1)}, f32[2048]{0:T(1024)}, u32[]{:S(2)}) copy-start(f32[2048]{0:T(1024)} %param.18) | copy-start | bytes 24580
  40.3 2.0 copy-start
  40.3 4.1 %copy-start.17 = (bf16[256,1408]{1,0:T(8,128)(2,1)S(1)}, bf16[256,1408]{1,0:T(8,128)(2,1)}, u32[]{:S(2)}) copy-start(bf16[256,1408]{1,0:T(8,128)(2,1)} %refs_9_.1) | copy-start | bytes 2162692
  42.3 19.1 %collective-permute-start.5 = (bf16[256,1408]{1,0:T(8,128)(2,1)S(1)}, bf16[256,1408]{1,0:T(8,128)(2,1)S(1)}, u32[]{:S(2)}, u32[]{:S(2)}) collective-permute-start(bf16[256,1408]{1,0:T(8,128)(2,1)S(1)} %copy-done), channel_id=1, source_target_pairs={{0,8},{8,16},{16,24},{24,28},{28,20},{20,12},{12,4},{4,0},{1,9},{9... | collective-permute-start | bytes 2162696 | tf_op jit(solution)/shard_map/ppermute | solution.py:146
  44.0 19.0 %collective-permute-start.6 = (bf16[256,1408]{1,0:T(8,128)(2,1)S(1)}, bf16[256,1408]{1,0:T(8,128)(2,1)S(1)}, u32[]{:S(2)}, u32[]{:S(2)}) collective-permute-start(bf16[256,1408]{1,0:T(8,128)(2,1)S(1)} %copy-done), channel_id=1, source_target_pairs={{8,0},{16,8},{24,16},{28,24},{20,28},{12,20},{4,12},{0,4},{9,1},{1... | collective-permute-start | bytes 2162696 | tf_op jit(solution)/shard_map/ppermute | solution.py:147
  44.4 32.4 %collective-permute-start.13 = (bf16[256,1408]{1,0:T(8,128)(2,1)S(1)}, bf16[256,1408]{1,0:T(8,128)(2,1)S(1)}, u32[]{:S(2)}, u32[]{:S(2)}) collective-permute-start(bf16[256,1408]{1,0:T(8,128)(2,1)S(1)} %copy-done.17), channel_id=1, source_target_pairs={{0,8},{8,16},{16,24},{24,28},{28,20},{20,12},{12,4},{4,0},{1,9},{9... | collective-permute-start | bytes 2162696 | tf_op jit(solution)/shard_map/ppermute | solution.py:146
  46.0 32.4 %collective-permute-start.14 = (bf16[256,1408]{1,0:T(8,128)(2,1)S(1)}, bf16[256,1408]{1,0:T(8,128)(2,1)S(1)}, u32[]{:S(2)}, u32[]{:S(2)}) collective-permute-start(bf16[256,1408]{1,0:T(8,128)(2,1)S(1)} %copy-done.17), channel_id=1, source_target_pairs={{8,0},{16,8},{24,16},{28,24},{20,28},{12,20},{4,12},{0,4},{9,1},{1... | collective-permute-start | bytes 2162696 | tf_op jit(solution)/shard_map/ppermute | solution.py:147
  46.4 47.4 %collective-permute-start.22 = (bf16[1408,256]{1,0:T(8,128)(2,1)}, bf16[1408,256]{1,0:T(8,128)(2,1)S(1)}, u32[]{:S(2)}, u32[]{:S(2)}) collective-permute-start(bf16[1408,256]{1,0:T(8,128)(2,1)} %param.21), channel_id=1, source_target_pairs={{8,0},{16,8},{24,16},{28,24},{20,28},{12,20},{4,12},{0,4},{9,1},{1... | collective-permute-start | bytes 2162696 | tf_op jit(solution)/shard_map/ppermute | solution.py:147
  61.4 32.9 %collective-permute-start.21 = (bf16[1408,256]{1,0:T(8,128)(2,1)}, bf16[1408,256]{1,0:T(8,128)(2,1)S(1)}, u32[]{:S(2)}, u32[]{:S(2)}) collective-permute-start(bf16[1408,256]{1,0:T(8,128)(2,1)} %param.21), channel_id=1, source_target_pairs={{0,8},{8,16},{16,24},{24,28},{28,20},{20,12},{12,4},{4,0},{1,9},{9... | collective-permute-start | bytes 2162696 | tf_op jit(solution)/shard_map/ppermute | solution.py:146
  63.0 44.8 %collective-permute-start.7 = (bf16[256,1408]{1,0:T(8,128)(2,1)S(1)}, bf16[256,1408]{1,0:T(8,128)(2,1)S(1)}, u32[]{:S(2)}, u32[]{:S(2)}) collective-permute-start(bf16[256,1408]{1,0:T(8,128)(2,1)S(1)} %collective-permute-done.5.refs_1_), channel_id=1, source_target_pairs={{0,8},{8,16},{16,24},{24,28},{28,20},{20,12},{12,4},{4,0},{1,9},{9... | collective-permute-start | bytes 2162696 | tf_op jit(solution)/shard_map/ppermute | solution.py:146
  76.8 77.2 %copy-start.23 = (bf16[256,1408]{1,0:T(8,128)(2,1)}, bf16[256,1408]{1,0:T(8,128)(2,1)S(1)}, u32[]{:S(2)}) copy-start(bf16[256,1408]{1,0:T(8,128)(2,1)S(1)} %collective-permute-done.13.refs_10_) | copy-start | bytes 2162692
  76.8 32.5 %collective-permute-start.8 = (bf16[256,1408]{1,0:T(8,128)(2,1)S(1)}, bf16[256,1408]{1,0:T(8,128)(2,1)S(1)}, u32[]{:S(2)}, u32[]{:S(2)}) collective-permute-start(bf16[256,1408]{1,0:T(8,128)(2,1)S(1)} %collective-permute-done.6.refs_2_), channel_id=1, source_target_pairs={{8,0},{16,8},{24,16},{28,24},{20,28},{12,20},{4,12},{0,4},{9,1},{1... | collective-permute-start | bytes 2162696 | tf_op jit(solution)/shard_map/ppermute | solution.py:147
  78.4 75.7 %copy-start.24 = (bf16[256,1408]{1,0:T(8,128)(2,1)}, bf16[256,1408]{1,0:T(8,128)(2,1)S(1)}, u32[]{:S(2)}) copy-start(bf16[256,1408]{1,0:T(8,128)(2,1)S(1)} %collective-permute-done.14.refs_11_) | copy-start | bytes 2162692
  78.4 44.8 %collective-permute-start.15 = (bf16[256,1408]{1,0:T(8,128)(2,1)S(1)}, bf16[256,1408]{1,0:T(8,128)(2,1)S(1)}, u32[]{:S(2)}, u32[]{:S(2)}) collective-permute-start(bf16[256,1408]{1,0:T(8,128)(2,1)S(1)} %collective-permute-done.13.refs_10_), channel_id=1, source_target_pairs={{0,8},{8,16},{16,24},{24,28},{28,20},{20,12},{12,4},{4,0},{1,9},{9... | collective-permute-start | bytes 2162696 | tf_op jit(solution)/shard_map/ppermute | solution.py:146
  93.9 60.2 %copy-start.19 = (bf16[1408,256]{1,0:T(8,128)(2,1)}, bf16[1408,256]{1,0:T(8,128)(2,1)S(1)}, u32[]{:S(2)}) copy-start(bf16[1408,256]{1,0:T(8,128)(2,1)S(1)} %collective-permute-done.22) | copy-start | bytes 2162692
  93.9 31.7 %collective-permute-start.16 = (bf16[256,1408]{1,0:T(8,128)(2,1)S(1)}, bf16[256,1408]{1,0:T(8,128)(2,1)S(1)}, u32[]{:S(2)}, u32[]{:S(2)}) collective-permute-start(bf16[256,1408]{1,0:T(8,128)(2,1)S(1)} %collective-permute-done.14.refs_11_), channel_id=1, source_target_pairs={{8,0},{16,8},{24,16},{28,24},{20,28},{12,20},{4,12},{0,4},{9,1},{1... | collective-permute-start | bytes 2162696 | tf_op jit(solution)/shard_map/ppermute | solution.py:147
  94.3 59.8 %copy-start.21 = (bf16[1408,256]{1,0:T(8,128)(2,1)}, bf16[1408,256]{1,0:T(8,128)(2,1)S(1)}, u32[]{:S(2)}) copy-start(bf16[1408,256]{1,0:T(8,128)(2,1)S(1)} %collective-permute-done.21) | copy-start | bytes 2162692
  94.3 46.0 %collective-permute-start.27 = (bf16[1408,256]{1,0:T(8,128)(2,1)S(1)}, bf16[1408,256]{1,0:T(8,128)(2,1)}, u32[]{:S(2)}, u32[]{:S(2)}) collective-permute-start(bf16[1408,256]{1,0:T(8,128)(2,1)S(1)} %collective-permute-done.22), channel_id=1, source_target_pairs={{8,0},{16,8},{24,16},{28,24},{20,28},{12,20},{4,12},{0,4},{9,1},{1... | collective-permute-start | bytes 2162696 | tf_op jit(solution)/shard_map/ppermute | solution.py:147
  107.7 33.0 %collective-permute-start.26 = (bf16[1408,256]{1,0:T(8,128)(2,1)S(1)}, bf16[1408,256]{1,0:T(8,128)(2,1)S(1)}, u32[]{:S(2)}, u32[]{:S(2)}) collective-permute-start(bf16[1408,256]{1,0:T(8,128)(2,1)S(1)} %collective-permute-done.21), channel_id=1, source_target_pairs={{0,8},{8,16},{16,24},{24,28},{28,20},{20,12},{12,4},{4,0},{1,9},{9... | collective-permute-start | bytes 2162696 | tf_op jit(solution)/shard_map/ppermute | solution.py:146
  109.3 44.8 %collective-permute-start.9 = (bf16[256,1408]{1,0:T(8,128)(2,1)S(1)}, bf16[256,1408]{1,0:T(8,128)(2,1)S(1)}, u32[]{:S(2)}, u32[]{:S(2)}) collective-permute-start(bf16[256,1408]{1,0:T(8,128)(2,1)S(1)} %collective-permute-done.7.refs_3_), channel_id=1, source_target_pairs={{0,8},{8,16},{16,24},{24,28},{28,20},{20,12},{12,4},{4,0},{1,9},{9... | collective-permute-start | bytes 2162696 | tf_op jit(solution)/shard_map/ppermute | solution.py:146
  123.2 61.9 %copy-start.27 = (bf16[256,1408]{1,0:T(8,128)(2,1)}, bf16[256,1408]{1,0:T(8,128)(2,1)S(1)}, u32[]{:S(2)}) copy-start(bf16[256,1408]{1,0:T(8,128)(2,1)S(1)} %collective-permute-done.15.refs_12_) | copy-start | bytes 2162692
  123.2 33.3 %collective-permute-start.10 = (bf16[256,1408]{1,0:T(8,128)(2,1)S(1)}, bf16[256,1408]{1,0:T(8,128)(2,1)S(1)}, u32[]{:S(2)}, u32[]{:S(2)}) collective-permute-start(bf16[256,1408]{1,0:T(8,128)(2,1)S(1)} %collective-permute-done.8.refs_4_), channel_id=1, source_target_pairs={{8,0},{16,8},{24,16},{28,24},{20,28},{12,20},{4,12},{0,4},{9,1},{1... | collective-permute-start | bytes 2162696 | tf_op jit(solution)/shard_map/ppermute | solution.py:147
  125.6 59.5 %copy-start.28 = (bf16[256,1408]{1,0:T(8,128)(2,1)}, bf16[256,1408]{1,0:T(8,128)(2,1)S(1)}, u32[]{:S(2)}) copy-start(bf16[256,1408]{1,0:T(8,128)(2,1)S(1)} %collective-permute-done.16.refs_13_) | copy-start | bytes 2162692
  125.6 43.9 %collective-permute-start.17 = (bf16[256,1408]{1,0:T(8,128)(2,1)S(1)}, bf16[256,1408]{1,0:T(8,128)(2,1)S(1)}, u32[]{:S(2)}, u32[]{:S(2)}) collective-permute-start(bf16[256,1408]{1,0:T(8,128)(2,1)S(1)} %collective-permute-done.15.refs_12_), channel_id=1, source_target_pairs={{0,8},{8,16},{16,24},{24,28},{28,20},{20,12},{12,4},{4,0},{1,9},{9... | collective-permute-start | bytes 2162696 | tf_op jit(solution)/shard_map/ppermute | solution.py:146
  140.3 31.5 %collective-permute-start.18 = (bf16[256,1408]{1,0:T(8,128)(2,1)S(1)}, bf16[256,1408]{1,0:T(8,128)(2,1)S(1)}, u32[]{:S(2)}, u32[]{:S(2)}) collective-permute-start(bf16[256,1408]{1,0:T(8,128)(2,1)S(1)} %collective-permute-done.16.refs_13_), channel_id=1, source_target_pairs={{8,0},{16,8},{24,16},{28,24},{20,28},{12,20},{4,12},{0,4},{9,1},{1... | collective-permute-start | bytes 2162696 | tf_op jit(solution)/shard_map/ppermute | solution.py:147
  140.8 32.8 %copy-start.25 = (bf16[1408,256]{1,0:T(8,128)(2,1)}, bf16[1408,256]{1,0:T(8,128)(2,1)S(1)}, u32[]{:S(2)}) copy-start(bf16[1408,256]{1,0:T(8,128)(2,1)S(1)} %collective-permute-done.26) | copy-start | bytes 2162692
  140.8 44.3 %collective-permute-start.31 = (bf16[1408,256]{1,0:T(8,128)(2,1)S(1)}, bf16[1408,256]{1,0:T(8,128)(2,1)}, u32[]{:S(2)}, u32[]{:S(2)}) collective-permute-start(bf16[1408,256]{1,0:T(8,128)(2,1)S(1)} %collective-permute-done.26), channel_id=1, source_target_pairs={{0,8},{8,16},{16,24},{24,28},{28,20},{20,12},{12,4},{4,0},{1,9},{9... | collective-permute-start | bytes 2162696 | tf_op jit(solution)/shard_map/ppermute | solution.py:146
  154.1 47.8 %collective-permute-start.32 = (bf16[1408,256]{1,0:T(8,128)(2,1)}, bf16[1408,256]{1,0:T(8,128)(2,1)}, u32[]{:S(2)}, u32[]{:S(2)}) collective-permute-start(bf16[1408,256]{1,0:T(8,128)(2,1)} %collective-permute-done.27), channel_id=1, source_target_pairs={{8,0},{16,8},{24,16},{28,24},{20,28},{12,20},{4,12},{0,4},{9,1},{1... | collective-permute-start | bytes 2162696 | tf_op jit(solution)/shard_map/ppermute | solution.py:147
  156.5 47.7 %collective-permute-start.11 = (bf16[128,1408]{1,0:T(8,128)(2,1)}, bf16[128,1408]{1,0:T(8,128)(2,1)S(1)}, u32[]{:S(2)}, u32[]{:S(2)}) collective-permute-start(bf16[128,1408]{1,0:T(8,128)(2,1)} %slice.149), channel_id=1, source_target_pairs={{0,8},{8,16},{16,24},{24,28},{28,20},{20,12},{12,4},{4,0},{1,9},{9... | collective-permute-start | bytes 1081352 | tf_op jit(solution)/shard_map/ppermute | solution.py:150
  169.5 1.5 copy-start.12
  169.5 36.2 %collective-permute-start.12 = (bf16[128,1408]{1,0:T(8,128)(2,1)}, bf16[128,1408]{1,0:T(8,128)(2,1)}, u32[]{:S(2)}, u32[]{:S(2)}) collective-permute-start(bf16[128,1408]{1,0:T(8,128)(2,1)} %slice.150), channel_id=1, source_target_pairs={{8,0},{16,8},{24,16},{28,24},{20,28},{12,20},{4,12},{0,4},{9,1},{1... | collective-permute-start | bytes 1081352 | tf_op jit(solution)/shard_map/ppermute | solution.py:151
  171.9 33.9 %collective-permute-start.19 = (bf16[128,1408]{1,0:T(8,128)(2,1)}, bf16[128,1408]{1,0:T(8,128)(2,1)}, u32[]{:S(2)}, u32[]{:S(2)}) collective-permute-start(bf16[128,1408]{1,0:T(8,128)(2,1)} %slice.151), channel_id=1, source_target_pairs={{0,8},{8,16},{16,24},{24,28},{28,20},{20,12},{12,4},{4,0},{1,9},{9... | collective-permute-start | bytes 1081352 | tf_op jit(solution)/shard_map/ppermute | solution.py:150
  185.1 20.6 %collective-permute-start.20 = (bf16[128,1408]{1,0:T(8,128)(2,1)}, bf16[128,1408]{1,0:T(8,128)(2,1)}, u32[]{:S(2)}, u32[]{:S(2)}) collective-permute-start(bf16[128,1408]{1,0:T(8,128)(2,1)} %slice.152), channel_id=1, source_target_pairs={{8,0},{16,8},{24,16},{28,24},{20,28},{12,20},{4,12},{0,4},{9,1},{1... | collective-permute-start | bytes 1081352 | tf_op jit(solution)/shard_map/ppermute | solution.py:151
  201.9 34.4 %collective-permute-start.36 = (bf16[704,256]{1,0:T(8,128)(2,1)}, bf16[704,256]{1,0:T(8,128)(2,1)}, u32[]{:S(2)}, u32[]{:S(2)}) collective-permute-start(bf16[704,256]{1,0:T(8,128)(2,1)} %slice.160), channel_id=1, source_target_pairs={{0,8},{8,16},{16,24},{24,28},{28,20},{20,12},{12,4},{4,0},{1,9},{9... | collective-permute-start | bytes 1081352 | tf_op jit(solution)/shard_map/ppermute | solution.py:150
  204.2 32.4 %collective-permute-start.37 = (bf16[704,256]{1,0:T(8,128)(2,1)}, bf16[704,256]{1,0:T(8,128)(2,1)}, u32[]{:S(2)}, u32[]{:S(2)}) collective-permute-start(bf16[704,256]{1,0:T(8,128)(2,1)} %slice.161), channel_id=1, source_target_pairs={{8,0},{16,8},{24,16},{28,24},{20,28},{12,20},{4,12},{0,4},{9,1},{1... | collective-permute-start | bytes 1081352 | tf_op jit(solution)/shard_map/ppermute | solution.py:151
  205.8 1.1 copy-start.2
  208.0 15.1 %copy-start.18 = (bf16[1408,256]{1,0:T(8,128)(2,1)S(1)}, bf16[1408,256]{1,0:T(8,128)(2,1)}, u32[]{:S(2)}) copy-start(bf16[1408,256]{1,0:T(8,128)(2,1)} %param.21) | copy-start | bytes 2162692
  223.1 2.5 copy-start.29
  229.5 10.7 %collective-permute-start.33 = (bf16[192,512]{1,0:T(8,128)(2,1)S(1)}, bf16[192,512]{1,0:T(8,128)(2,1)S(1)}, u32[]{:S(2)}, u32[]{:S(2)}) collective-permute-start(bf16[192,512]{1,0:T(8,128)(2,1)S(1)} %get-tuple-element.8), channel_id=1, source_target_pairs={{0,1},{1,2},{2,3},{3,0},{4,5},{5,6},{6,7},{7,4},{8,9},{9,10},{10,1... | collective-permute-start | bytes 589832 | tf_op jit(solution)/shard_map/ppermute | solution.py:118
  229.6 12.1 %collective-permute-start.34 = (bf16[192,512]{1,0:T(8,128)(2,1)S(1)}, bf16[192,512]{1,0:T(8,128)(2,1)S(1)}, u32[]{:S(2)}, u32[]{:S(2)}) collective-permute-start(bf16[192,512]{1,0:T(8,128)(2,1)S(1)} %get-tuple-element.9), channel_id=1, source_target_pairs={{0,2},{1,3},{2,0},{3,1},{4,6},{5,7},{6,4},{7,5},{8,10},{9,11},{10,... | collective-permute-start | bytes 589832 | tf_op jit(solution)/shard_map/ppermute | solution.py:118
  230.2 3.0 %copy-start.26 = (bf16[1408,256]{1,0:T(8,128)(2,1)S(1)}, bf16[1408,256]{1,0:T(8,128)(2,1)}, u32[]{:S(2)}) copy-start(bf16[1408,256]{1,0:T(8,128)(2,1)} %copy-done.25) | copy-start | bytes 2162692
  230.2 11.5 %collective-permute-start.35 = (bf16[192,512]{1,0:T(8,128)(2,1)S(1)}, bf16[192,512]{1,0:T(8,128)(2,1)S(1)}, u32[]{:S(2)}, u32[]{:S(2)}) collective-permute-start(bf16[192,512]{1,0:T(8,128)(2,1)S(1)} %get-tuple-element.10), channel_id=1, source_target_pairs={{0,3},{1,0},{2,1},{3,2},{4,7},{5,4},{6,5},{7,6},{8,11},{9,8},{10,9... | collective-permute-start | bytes 589832 | tf_op jit(solution)/shard_map/ppermute | solution.py:118
  233.2 1.1 copy-start.20
  236.3 8.2 %collective-permute-start.28 = (bf16[192,512]{1,0:T(8,128)(2,1)S(1)}, bf16[192,512]{1,0:T(8,128)(2,1)S(1)}, u32[]{:S(2)}, u32[]{:S(2)}) collective-permute-start(bf16[192,512]{1,0:T(8,128)(2,1)S(1)} %get-tuple-element.11), channel_id=1, source_target_pairs={{0,1},{1,2},{2,3},{3,0},{4,5},{5,6},{6,7},{7,4},{8,9},{9,10},{10,1... | collective-permute-start | bytes 589832 | tf_op jit(solution)/shard_map/ppermute | solution.py:118
  236.6 9.3 %collective-permute-start.29 = (bf16[192,512]{1,0:T(8,128)(2,1)S(1)}, bf16[192,512]{1,0:T(8,128)(2,1)S(1)}, u32[]{:S(2)}, u32[]{:S(2)}) collective-permute-start(bf16[192,512]{1,0:T(8,128)(2,1)S(1)} %get-tuple-element.12), channel_id=1, source_target_pairs={{0,2},{1,3},{2,0},{3,1},{4,6},{5,7},{6,4},{7,5},{8,10},{9,11},{10,... | collective-permute-start | bytes 589832 | tf_op jit(solution)/shard_map/ppermute | solution.py:118
  240.2 8.4 %collective-permute-start.30 = (bf16[192,512]{1,0:T(8,128)(2,1)S(1)}, bf16[192,512]{1,0:T(8,128)(2,1)S(1)}, u32[]{:S(2)}, u32[]{:S(2)}) collective-permute-start(bf16[192,512]{1,0:T(8,128)(2,1)S(1)} %get-tuple-element.13), channel_id=1, source_target_pairs={{0,3},{1,0},{2,1},{3,2},{4,7},{5,4},{6,5},{7,6},{8,11},{9,8},{10,9... | collective-permute-start | bytes 589832 | tf_op jit(solution)/shard_map/ppermute | solution.py:118
  241.6 13.4 %collective-permute-start.23 = (bf16[192,768]{1,0:T(8,128)(2,1)S(1)}, bf16[192,768]{1,0:T(8,128)(2,1)S(1)}, u32[]{:S(2)}, u32[]{:S(2)}) collective-permute-start(bf16[192,768]{1,0:T(8,128)(2,1)S(1)} %get-tuple-element.5), channel_id=1, source_target_pairs={{0,1},{1,2},{2,3},{3,0},{4,5},{5,6},{6,7},{7,4},{8,9},{9,10},{10,1... | collective-permute-start | bytes 884744 | tf_op jit(solution)/shard_map/ppermute | solution.py:118
  241.6 14.7 %collective-permute-start.24 = (bf16[192,768]{1,0:T(8,128)(2,1)S(1)}, bf16[192,768]{1,0:T(8,128)(2,1)S(1)}, u32[]{:S(2)}, u32[]{:S(2)}) collective-permute-start(bf16[192,768]{1,0:T(8,128)(2,1)S(1)} %get-tuple-element.7), channel_id=1, source_target_pairs={{0,2},{1,3},{2,0},{3,1},{4,6},{5,7},{6,4},{7,5},{8,10},{9,11},{10,... | collective-permute-start | bytes 884744 | tf_op jit(solution)/shard_map/ppermute | solution.py:118
  244.5 15.8 %collective-permute-start.25 = (bf16[192,768]{1,0:T(8,128)(2,1)S(1)}, bf16[192,768]{1,0:T(8,128)(2,1)S(1)}, u32[]{:S(2)}, u32[]{:S(2)}) collective-permute-start(bf16[192,768]{1,0:T(8,128)(2,1)S(1)} %get-tuple-element.6), channel_id=1, source_target_pairs={{0,3},{1,0},{2,1},{3,2},{4,7},{5,4},{6,5},{7,6},{8,11},{9,8},{10,9... | collective-permute-start | bytes 884744 | tf_op jit(solution)/shard_map/ppermute | solution.py:118
  244.6 15.9 %copy-start.7 = (bf16[192,2048]{1,0:T(8,128)(2,1)S(1)}, bf16[192,2048]{1,0:T(8,128)(2,1)}, u32[]{:S(2)}) copy-start(bf16[192,2048]{1,0:T(8,128)(2,1)} %copy.60) | copy-start | bytes 2359300
  244.6 15.9 %copy-start.6 = (bf16[192,2048]{1,0:T(8,128)(2,1)S(1)}, bf16[192,2048]{1,0:T(8,128)(2,1)}, u32[]{:S(2)}) copy-start(bf16[192,2048]{1,0:T(8,128)(2,1)} %copy-done.5) | copy-start | bytes 2359300
  245.8 17.6 %collective-permute-start.38 = (bf16[192,256]{1,0:T(8,128)(2,1)S(1)}, bf16[192,256]{1,0:T(8,128)(2,1)S(1)}, u32[]{:S(2)}, u32[]{:S(2)}) collective-permute-start(bf16[192,256]{1,0:T(8,128)(2,1)S(1)} %get-tuple-element.14), channel_id=1, source_target_pairs={{0,1},{1,2},{2,3},{3,0},{4,5},{5,6},{6,7},{7,4},{8,9},{9,10},{10,1... | collective-permute-start | bytes 294920 | tf_op jit(solution)/shard_map/ppermute | solution.py:118
  248.6 16.2 %collective-permute-start.39 = (bf16[192,256]{1,0:T(8,128)(2,1)S(1)}, bf16[192,256]{1,0:T(8,128)(2,1)S(1)}, u32[]{:S(2)}, u32[]{:S(2)}) collective-permute-start(bf16[192,256]{1,0:T(8,128)(2,1)S(1)} %get-tuple-element.16), channel_id=1, source_target_pairs={{0,2},{1,3},{2,0},{3,1},{4,6},{5,7},{6,4},{7,5},{8,10},{9,11},{10,... | collective-permute-start | bytes 294920 | tf_op jit(solution)/shard_map/ppermute | solution.py:118
  255.1 9.7 %collective-permute-start.40 = (bf16[192,256]{1,0:T(8,128)(2,1)S(1)}, bf16[192,256]{1,0:T(8,128)(2,1)S(1)}, u32[]{:S(2)}, u32[]{:S(2)}) collective-permute-start(bf16[192,256]{1,0:T(8,128)(2,1)S(1)} %get-tuple-element.15), channel_id=1, source_target_pairs={{0,3},{1,0},{2,1},{3,2},{4,7},{5,4},{6,5},{7,6},{8,11},{9,8},{10,9... | collective-permute-start | bytes 294920 | tf_op jit(solution)/shard_map/ppermute | solution.py:118
  260.8 4.0 %copy-start.8 = (bf16[192,2048]{1,0:T(8,128)(2,1)}, bf16[192,2048]{1,0:T(8,128)(2,1)S(1)}, u32[]{:S(2)}) copy-start(bf16[192,2048]{1,0:T(8,128)(2,1)S(1)} %fusion.49) | copy-start | bytes 2359300
  (8 other events, 7.6 us)
Sparse Core Ops, SparseCore 0:
  42.4 29.2 all-gather.1

commit v3 on v2

--- a/solution.py
+++ b/solution.py
@@ -1,3 +1,5 @@
+import functools
+
 import jax
 import jax.numpy as jnp
 from jax import lax
@@ -53,7 +55,8 @@
     return list(range(0, count, 2)) + list(range(1, count, 2))[::-1]
 
 
-def widen_body(starts, normed, *refs):
+def widen_body(parts, starts, *refs):
+    normed, refs = refs[:parts], refs[parts:]
     count = (len(refs) - 2) // 2
     gates, ups = refs[:count], refs[count : 2 * count]
     hidden, ordered = refs[-2:]
@@ -61,7 +64,11 @@
     for at, ref in enumerate(gates):
         depth = ref.shape[0]
         first = pl.multiple_of(starts[at], LANES)
-        ordered[:, base : base + depth] = normed[:, pl.ds(first, depth)]
+        for part, block in enumerate(normed):
+            size = block.shape[0]
+            ordered[part * size : (part + 1) * size, base : base + depth] = block[
+                :, pl.ds(first, depth)
+            ]
         base += depth
     total = hidden.shape[1]
     rows = ordered[...]
@@ -81,18 +88,17 @@
 
 
 def widened(normed, gates, ups, starts):
-    rows, depth = normed.shape
+    rows, depth = len(normed) * normed[0].shape[0], normed[0].shape[1]
     total = gates[0].shape[1]
-    tile = 256 if rows % 256 == 0 else rows
-    fixed = [pl.BlockSpec(block.shape, lambda i, s: (0, 0)) for block in gates + ups]
+    operands = [*normed, *gates, *ups]
     return pl.pallas_call(
-        widen_body,
+        functools.partial(widen_body, len(normed)),
         grid_spec=pltpu.PrefetchScalarGridSpec(
             num_scalar_prefetch=1,
-            grid=(rows // tile,),
-            in_specs=[pl.BlockSpec((tile, depth), lambda i, s: (i, 0))] + fixed,
-            out_specs=pl.BlockSpec((tile, total), lambda i, s: (i, 0)),
-            scratch_shapes=[pltpu.VMEM((tile, depth), jnp.bfloat16)],
+            grid=(1,),
+            in_specs=[pl.BlockSpec(block.shape, lambda i, s: (0, 0)) for block in operands],
+            out_specs=pl.BlockSpec((rows, total), lambda i, s: (0, 0)),
+            scratch_shapes=[pltpu.VMEM((rows, depth), jnp.bfloat16)],
         ),
         out_shape=jax.ShapeDtypeStruct((rows, total), jnp.bfloat16),
         compiler_params=pltpu.CompilerParams(
@@ -103,25 +109,54 @@
             transcendentals=rows * total,
             bytes_accessed=4 * depth * total + 2 * rows * (depth + total),
         ),
-    )(starts, normed, *gates, *ups)
+    )(starts, *operands)
+
+
+def rotated(block, step):
+    count = lax.axis_size("tp")
+    if step == 0:
+        return block
+    return lax.ppermute(block, "tp", [(i, (i + step) % count) for i in range(count)])
+
+
+def source(step):
+    count = lax.axis_size("tp")
+    return (lax.axis_index("tp").astype(jnp.uint32) + count - step) % count
 
 
 def exchanged(blocks):
     count = lax.axis_size("tp")
-    me = lax.axis_index("tp").astype(jnp.uint32)
     size = blocks.shape[0] // count
     pairs = []
     for step in range(count):
-        there = (me + step) % count
-        block = lax.dynamic_slice_in_dim(blocks, there * size, size, 0)
-        if step:
-            block = lax.ppermute(block, "tp", [(i, (i + step) % count) for i in range(count)])
-        pairs.append(((me + count - step) % count, block))
+        block = lax.dynamic_slice_in_dim(blocks, source(count - step) * size, size, 0)
+        pairs.append((source(step), rotated(block, step)))
     return pairs
 
 
 def uses_ring(count, widths):
     return count > 1 and count % 2 == 0 and min(widths) >= LANES
+
+
+def ring_table(count):
+    order = ring_order(count)
+    place = [order.index(dev) for dev in range(count)]
+    return [[order[(place[dev] + step) % count] for step in range(count)] for dev in range(count)]
+
+
+def piece_starts(axis, depth, pieces):
+    count = lax.axis_size(axis)
+    if pieces == 1:
+        return jnp.zeros((1,), jnp.int32)
+    steps = [0]
+    for step in range(1, count // 2):
+        steps += [-step, step]
+    rows = [
+        [around[step % count] * depth for step in steps]
+        + [around[count // 2] * depth, around[count // 2] * depth + depth // 2]
+        for around in ring_table(count)
+    ]
+    return jnp.array(rows, jnp.int32)[lax.axis_index(axis).astype(jnp.uint32)]
 
 
 def ring_hops(shard, axis, dim):
@@ -129,10 +164,7 @@
     if not uses_ring(count, (shard.shape[dim],)):
         return [[(jnp.uint32(0), 0, lax.all_gather(shard, axis, axis=dim, tiled=True))]]
     order = ring_order(count)
-    place = [0] * count
-    for at, dev in enumerate(order):
-        place[dev] = at
-    table = [[order[(place[dev] + step) % count] for step in range(count)] for dev in range(count)]
+    table = ring_table(count)
     owners = jnp.array(table, jnp.uint32)[lax.axis_index(axis)]
     ahead = [(order[i], order[(i + 1) % count]) for i in range(count)]
     back = [(dst, src) for src, dst in ahead]
@@ -187,11 +219,12 @@
     normed = (
         mixf * lax.rsqrt(jnp.mean(mixf * mixf, axis=-1, keepdims=True) + 1e-06) * norm_gain
     ).astype(jnp.bfloat16)
-    normed_all = lax.all_gather(normed, "tp", axis=0, tiled=True)
+    peers = lax.axis_size("tp")
+    normed_all = [rotated(normed, step) for step in range(peers)]
 
     depth = gate_hops[0][0][2].shape[0]
     pieces = [piece for hop in gate_hops for piece in hop]
-    starts = jnp.stack([owner.astype(jnp.int32) * depth + at for owner, at, _ in pieces])
+    starts = piece_starts("sp", depth, len(pieces))
     gates = [block for _, _, block in pieces]
     ups = [block for hop in up_hops for _, _, block in hop]
     hidden = widened(normed_all, gates, ups, starts)
@@ -209,7 +242,12 @@
             for _, block in group
         ]
         terms = jnp.concatenate(parts, axis=1)
-        ffn = sum(block.astype(jnp.float32) for _, block in exchanged(terms))
+        size = terms.shape[0] // peers
+        ffn = 0.0
+        for step in range(peers):
+            low = (peers - step) % peers * size
+            block = rotated(terms[low : low + size], step)
+            ffn = ffn + block.astype(jnp.float32)
         for at, (owner, block) in enumerate(group):
             width = block.shape[1]
             base = lax.dynamic_slice_in_dim(mixed, owner * width, width, 1).astype(jnp.float32)

time: 274 us -> 239 us (0.87)
  between operations: 24 us -> 5.79 us
  waiting for transfers between devices: 135 us -> 122 us
  local copies, waits for them, and re-layouts: 24.5 us -> 17.7 us
    ppermute x9, waiting for transfers between devices: 83.7 us -> 0.79 us  [ring_hops(): from_left = lax.ppermute(from_left, axis, ahead)]
    ppermute x9, waiting for transfers between devices: 27.9 us -> 96.7 us  [ring_hops(): from_right = lax.ppermute(from_right, axis, back)]
    ppermute x3, starting transfers between devices: 4.59 us -> 0.7 us  [ring_hops(): bottom = lax.ppermute(from_right[half:], axis, back)]
    unnamed x62 -> x48, local copies, waits for them, and re-layouts: 7.77 us -> 4.14 us
    ppermute x3, starting transfers between devices: 2.21 us -> 5.59 us  [ring_hops(): top = lax.ppermute(from_left[:half], axis, ahead)]
    ppermute x15 -> x18, starting transfers between devices: 12.3 us -> 14.9 us  [rotated(): lax.ppermute(block, 'tp', [(i, (i + step) % count) for i in range(count)])]
    ppermute x15 -> x18, waiting for transfers between devices: 22.9 us -> 22.7 us  [rotated(): lax.ppermute(block, 'tp', [(i, (i + step) % count) for i in range(count)])]
  transfers between devices with their start and end apart: 42 -> 44, of which waited for: 19 -> 20; matrix products, arithmetic and copies ran while one was open for 12% -> 16% of each run, Pallas kernels for 6% -> 7%
where the time goes in v3:
time: 239 us; the launch traced here: 237 us
  waiting for transfers between devices  122 us (51%)
  starting transfers between devices  51.8 us (22%)
  matrix products  19.6 us (8%)
  local copies, waits for them, and re-layouts  17.7 us (7%)
  Pallas kernels  15.9 us (7%)
  between operations  5.79 us (2%)
  other arithmetic  3.9 us (2%)
    ppermute x9, waiting for transfers between devices, ring_hops(): from_right = lax.ppermute(from_right, axis, back)  96.7 us
    ppermute x18, waiting for transfers between devices, rotated(): lax.ppermute(block, 'tp', [(i, (i + step) % count) for i in range(count)])  22.7 us
    ppermute x9, starting transfers between devices, ring_hops(): from_left = lax.ppermute(from_left, axis, ahead)  15.9 us
    pallas_call x1, Pallas kernels, widened(): pl.pallas_call(functools.partial(widen_body, len(normed)), grid_spec=pltp...  15.9 us
    ppermute x18, starting transfers between devices, rotated(): lax.ppermute(block, 'tp', [(i, (i + step) % count) for i in range(count)])  14.9 us
    dot_general x8, matrix products, shards(): jnp.dot(hidden, block, preferred_element_type=jnp.float32)  12.5 us
    ppermute x9, starting transfers between devices, ring_hops(): from_right = lax.ppermute(from_right, axis, back)  7.41 us
    ppermute x2, starting transfers between devices, passed_along(): return lax.ppermute(block, axis, route)  7.27 us
  transfers between devices with their start and end apart: 44, of which 20 were waited for; matrix products, arithmetic and copies ran while one was open for 16% of the time, Pallas kernels for 7%

profile of v3, /device:TPU:0, one launch (start us, length us, event | category | flops | bytes accessed | tf_op | source)
XLA Modules:
  0.0 237.0 jit_solution(12761185257583559745)
XLA Ops:
  0.0 3.1 %collective-permute-start.8 = (bf16[256,1408]{1,0:T(8,128)(2,1)}, bf16[256,1408]{1,0:T(8,128)(2,1)S(1)}, u32[]{:S(2)}, u32[]{:S(2)}) collective-permute-start(bf16[256,1408]{1,0:T(8,128)(2,1)} %refs_4_.1), channel_id=1, source_target_pairs={{0,8},{8,16},{16,24},{24,28},{28,20},{20,12},{12,4},{4,0},{1,9},{9... | collective-permute-start | bytes 2162696 | tf_op jit(solution)/shard_map/ppermute | solution.py:178
  3.8 3.9 %collective-permute-start.1 = (bf16[128,64]{0,1:T(8,128)(2,1)S(1)}, bf16[128,64]{0,1:T(8,128)(2,1)S(1)}, u32[]{:S(2)}, u32[]{:S(2)}) collective-permute-start(bf16[128,64]{0,1:T(8,128)(2,1)S(1)} %slice.133), channel_id=1, source_target_pairs={{0,4},{4,8},{8,12},{12,16},{16,20},{20,24},{24,28},{1,5},{5,9},{9,... | collective-permute-start | bytes 49160 | tf_op jit(solution)/shard_map/ppermute | solution.py:19
  8.4 3.4 %collective-permute-start = (bf16[128,64]{0,1:T(8,128)(2,1)S(1)}, bf16[128,64]{0,1:T(8,128)(2,1)S(1)}, u32[]{:S(2)}, u32[]{:S(2)}) collective-permute-start(bf16[128,64]{0,1:T(8,128)(2,1)S(1)} %slice.131), channel_id=1, source_target_pairs={{0,4},{4,8},{8,12},{12,16},{16,20},{20,24},{24,28},{1,5},{5,9},{9,... | collective-permute-start | bytes 49160 | tf_op jit(solution)/shard_map/ppermute | solution.py:19
  11.8 1.6 collective-permute-start.16
  13.8 1.0 reshape.177
  14.9 1.0 reshape.174
  15.9 1.8 reshape.183
  17.8 1.4 collective-permute-done.1
  20.3 1.5 copy-done.5
  22.8 2.8 %fusion.12 = bf16[6,128,1,4,64]{1,4,3,0,2:T(8,128)(2,1)S(1)} fusion(f32[6,4,128]{2,1,0:T(4,128)S(1)} %exponential_add_fusion, f32[6,4,128]{2,1,0:T(4,128)S(1)} %broadcast_maximum_fusion, f32[6,256,128,4]{2,1,3,0:T(8,128)} %copy-done.5, pred[6,128,256]{1,2,0:T(8,128)(4,1)S(1)} %broadcast_and_fusion, bf16[6,128,1,64]{1,3,0,2:T(8,128)(2,1)S(1)} %copy.23, ...), kind=kOutput, calls=%fused_computation.24 | convolution fusion | flops 105185280 | bytes 3956736 | tf_op jit(solution)/shard_map/nhgqk,nkhd->nqhgd/dot_general | solution.py:50
  26.3 1.7 collective-permute-start.3
  28.0 3.4 %collective-permute-done.2 = bf16[192,256]{0,1:T(8,128)(2,1)S(1)} collective-permute-done((bf16[192,256]{0,1:T(8,128)(2,1)S(1)}, bf16[192,256]{0,1:T(8,128)(2,1)S(1)}, u32[]{:S(2)}, u32[]{:S(2)}) %collective-permute-start.2) | collective-permute-done | bytes 98336 | tf_op jit(solution)/shard_map/ppermute | solution.py:119
  31.4 1.3 collective-permute-done.3
  32.8 2.5 %collective-permute-start.17 = (bf16[256,1408]{1,0:T(8,128)(2,1)}, bf16[256,1408]{1,0:T(8,128)(2,1)}, u32[]{:S(2)}, u32[]{:S(2)}) collective-permute-start(bf16[256,1408]{1,0:T(8,128)(2,1)} %refs_13_.1), channel_id=1, source_target_pairs={{8,0},{16,8},{24,16},{28,24},{20,28},{12,20},{4,12},{0,4},{9,1},{1... | collective-permute-start | bytes 2162696 | tf_op jit(solution)/shard_map/ppermute | solution.py:179
  35.2 1.3 collective-permute-start.25
  36.5 1.0 collective-permute-start.24
  37.6 2.0 collective-permute-start.10
  39.6 14.0 %collective-permute-done.17.refs_15_ = bf16[256,1408]{1,0:T(8,128)(2,1)} collective-permute-done((bf16[256,1408]{1,0:T(8,128)(2,1)}, bf16[256,1408]{1,0:T(8,128)(2,1)}, u32[]{:S(2)}, u32[]{:S(2)}) %collective-permute-start.17) | collective-permute-done | bytes 720928 | tf_op jit(solution)/shard_map/ppermute | solution.py:179
  53.6 2.0 collective-permute-start.18
  55.7 13.4 %collective-permute-done.25 = bf16[1408,256]{1,0:T(8,128)(2,1)} collective-permute-done((bf16[1408,256]{1,0:T(8,128)(2,1)}, bf16[1408,256]{1,0:T(8,128)(2,1)}, u32[]{:S(2)}, u32[]{:S(2)}) %collective-permute-start.25) | collective-permute-done | bytes 720928 | tf_op jit(solution)/shard_map/ppermute | solution.py:179
  69.1 0.9 collective-permute-start.19
  70.1 0.8 collective-permute-start.30
  70.9 1.3 collective-permute-start.29
  72.2 12.3 %collective-permute-done.11.refs_8_ = bf16[256,1408]{1,0:T(8,128)(2,1)} collective-permute-done((bf16[256,1408]{1,0:T(8,128)(2,1)S(1)}, bf16[256,1408]{1,0:T(8,128)(2,1)}, u32[]{:S(2)}, u32[]{:S(2)}) %collective-permute-start.11) | collective-permute-done | bytes 720928 | tf_op jit(solution)/shard_map/ppermute | solution.py:179
  84.5 2.0 collective-permute-start.12
  86.6 3.5 %fusion.3 = (f32[192]{0:T(256)S(1)}, bf16[192,2048]{1,0:T(8,128)(2,1)S(1)}) fusion(bf16[192,1024]{0,1:T(8,128)(2,1)S(1)} %constant_dynamic-update-slice_fusion, bf16[1024,2048]{1,0:T(8,128)(2,1)} %param.17, bf16[192,2048]{1,0:T(8,128)(2,1)} %param.12), kind=kOutput, calls=%fused_computation.9 | convolution fusion | flops 807665472 | bytes 6161152 | tf_op jit(solution)/shard_map/dot_general | solution.py:216
  90.2 9.7 %collective-permute-done.19.refs_17_ = bf16[256,1408]{1,0:T(8,128)(2,1)S(1)} collective-permute-done((bf16[256,1408]{1,0:T(8,128)(2,1)}, bf16[256,1408]{1,0:T(8,128)(2,1)S(1)}, u32[]{:S(2)}, u32[]{:S(2)}) %collective-permute-start.19) | collective-permute-done | bytes 720928 | tf_op jit(solution)/shard_map/ppermute | solution.py:179
  99.9 2.0 collective-permute-start.20
  101.9 13.4 %collective-permute-done.30 = bf16[1408,256]{1,0:T(8,128)(2,1)S(1)} collective-permute-done((bf16[1408,256]{1,0:T(8,128)(2,1)}, bf16[1408,256]{1,0:T(8,128)(2,1)S(1)}, u32[]{:S(2)}, u32[]{:S(2)}) %collective-permute-start.30) | collective-permute-done | bytes 720928 | tf_op jit(solution)/shard_map/ppermute | solution.py:179
  115.3 0.9 collective-permute-start.21
  116.2 1.1 fusion.5.refs_0_
  117.4 1.7 collective-permute-start.6
  119.1 11.7 %collective-permute-done.13.refs_10_ = bf16[256,1408]{1,0:T(8,128)(2,1)S(1)} collective-permute-done((bf16[256,1408]{1,0:T(8,128)(2,1)}, bf16[256,1408]{1,0:T(8,128)(2,1)S(1)}, u32[]{:S(2)}, u32[]{:S(2)}) %collective-permute-start.13) | collective-permute-done | bytes 720928 | tf_op jit(solution)/shard_map/ppermute | solution.py:179
  130.8 0.9 collective-permute-start.35
  132.5 0.8 collective-permute-start.34
  133.3 13.0 %collective-permute-done.21.refs_19_ = bf16[256,1408]{1,0:T(8,128)(2,1)S(1)} collective-permute-done((bf16[256,1408]{1,0:T(8,128)(2,1)S(1)}, bf16[256,1408]{1,0:T(8,128)(2,1)S(1)}, u32[]{:S(2)}, u32[]{:S(2)}) %collective-permute-start.21) | collective-permute-done | bytes 720928 | tf_op jit(solution)/shard_map/ppermute | solution.py:179
  146.2 1.1 collective-permute-start.7
  150.4 1.5 collective-permute-start.14
  152.6 9.2 %collective-permute-done.35 = bf16[1408,256]{1,0:T(8,128)(2,1)} collective-permute-done((bf16[1408,256]{1,0:T(8,128)(2,1)S(1)}, bf16[1408,256]{1,0:T(8,128)(2,1)}, u32[]{:S(2)}, u32[]{:S(2)}) %collective-permute-start.35) | collective-permute-done | bytes 720928 | tf_op jit(solution)/shard_map/ppermute | solution.py:179
  161.8 2.0 collective-permute-start.22
  171.2 1.1 copy.60
  172.3 1.0 slice.199
  173.3 1.0 slice.200
  174.3 2.1 collective-permute-start.39
  177.1 15.9 %shard_map.118 = bf16[768,1408]{1,0:T(8,128)(2,1)} custom-call(s32[9]{0:T(128)S(1)} %dynamic-slice_bitcast_fusion.starts, bf16[192,2048]{1,0:T(8,128)(2,1)} %fusion.5.refs_0_, bf16[192,2048]{1,0:T(8,128)(2,1)} %copy-done.14, bf16[192,2048]{1,0:T(8,128)(2,1)} %copy-done.15, bf16[192,2048]{1,0:T(8,128)(2,1)} %collective-permute-done.7.refs_3_, ...), custom_call_target="tpu_custom_call" | custom-call | flops 8858370048 | bytes 16842752 | tf_op jit(solution)/shard_map/pallas_call | solution.py:94
  193.0 2.7 %convolution_convert_fusion.7 = bf16[768,256]{1,0:T(8,128)(2,1)S(1)} fusion(bf16[768,1408]{1,0:T(8,128)(2,1)} %shard_map.118, bf16[1408,256]{1,0:T(8,128)(2,1)} %param.21), kind=kOutput, calls=%fused_computation.22 | convolution fusion | flops 553844736 | bytes 3276800 | tf_op jit(solution)/shard_map/dot_general | solution.py:241
  195.7 1.9 convolution_convert_fusion.1
  197.6 1.9 convolution_convert_fusion.2
  199.6 1.6 collective-permute-start.37
  201.1 1.4 collective-permute-start.38
  202.5 1.9 convolution_convert_fusion.5
  204.4 1.9 convolution_convert_fusion.6
  206.4 1.0 copy-done.17
  210.9 1.4 collective-permute-start.33
  212.4 1.6 collective-permute-start.27
  213.9 2.1 collective-permute-done.31
  216.1 1.2 collective-permute-done.32
  217.4 2.7 %collective-permute-start.41 = (bf16[192,256]{1,0:T(8,128)(2,1)S(1)}, bf16[192,256]{1,0:T(8,128)(2,1)S(1)}, u32[]{:S(2)}, u32[]{:S(2)}) collective-permute-start(bf16[192,256]{1,0:T(8,128)(2,1)S(1)} %get-tuple-element.14), channel_id=1, source_target_pairs={{0,1},{1,2},{2,3},{3,0},{4,5},{5,6},{6,7},{7,4},{8,9},{9,10},{10,1... | collective-permute-start | bytes 294920 | tf_op jit(solution)/shard_map/ppermute | solution.py:119
  220.1 1.1 collective-permute-start.42
  221.2 5.3 %collective-permute-done.26 = bf16[192,768]{1,0:T(8,128)(2,1)S(1)} collective-permute-done((bf16[192,768]{1,0:T(8,128)(2,1)S(1)}, bf16[192,768]{1,0:T(8,128)(2,1)S(1)}, u32[]{:S(2)}, u32[]{:S(2)}) %collective-permute-start.26) | collective-permute-done | bytes 294944 | tf_op jit(solution)/shard_map/ppermute | solution.py:119
  226.6 1.3 collective-permute-done.27
  227.9 4.4 %collective-permute-done.28 = bf16[192,768]{1,0:T(8,128)(2,1)S(1)} collective-permute-done((bf16[192,768]{1,0:T(8,128)(2,1)S(1)}, bf16[192,768]{1,0:T(8,128)(2,1)S(1)}, u32[]{:S(2)}, u32[]{:S(2)}) %collective-permute-start.28) | collective-permute-done | bytes 294944 | tf_op jit(solution)/shard_map/ppermute | solution.py:119
  232.7 2.3 collective-permute-done.41
  235.0 1.3 collective-permute-done.42
  (139 shorter events, 17.0 us)
Async XLA Ops:
  0.0 19.2 %copy-start.7 = (bf16[768,64]{0,1:T(8,128)(2,1)S(1)}, bf16[768,64]{0,1:T(8,128)(2,1)}, u32[]{:S(2)}) copy-start(bf16[768,64]{0,1:T(8,128)(2,1)} %param.14) | copy-start | bytes 294916
  0.0 36.5 %collective-permute-start.8 = (bf16[256,1408]{1,0:T(8,128)(2,1)}, bf16[256,1408]{1,0:T(8,128)(2,1)S(1)}, u32[]{:S(2)}, u32[]{:S(2)}) collective-permute-start(bf16[256,1408]{1,0:T(8,128)(2,1)} %refs_4_.1), channel_id=1, source_target_pairs={{0,8},{8,16},{16,24},{24,28},{28,20},{20,12},{12,4},{4,0},{1,9},{9... | collective-permute-start | bytes 2162696 | tf_op jit(solution)/shard_map/ppermute | solution.py:178
  3.1 34.5 %collective-permute-start.9 = (bf16[256,1408]{1,0:T(8,128)(2,1)}, bf16[256,1408]{1,0:T(8,128)(2,1)S(1)}, u32[]{:S(2)}, u32[]{:S(2)}) collective-permute-start(bf16[256,1408]{1,0:T(8,128)(2,1)} %refs_4_.1), channel_id=1, source_target_pairs={{8,0},{16,8},{24,16},{28,24},{20,28},{12,20},{4,12},{0,4},{9,1},{1... | collective-permute-start | bytes 2162696 | tf_op jit(solution)/shard_map/ppermute | solution.py:179
  3.8 15.4 %collective-permute-start.1 = (bf16[128,64]{0,1:T(8,128)(2,1)S(1)}, bf16[128,64]{0,1:T(8,128)(2,1)S(1)}, u32[]{:S(2)}, u32[]{:S(2)}) collective-permute-start(bf16[128,64]{0,1:T(8,128)(2,1)S(1)} %slice.133), channel_id=1, source_target_pairs={{0,4},{4,8},{8,12},{12,16},{16,20},{20,24},{24,28},{1,5},{5,9},{9,... | collective-permute-start | bytes 49160 | tf_op jit(solution)/shard_map/ppermute | solution.py:19
  8.4 14.2 %collective-permute-start = (bf16[128,64]{0,1:T(8,128)(2,1)S(1)}, bf16[128,64]{0,1:T(8,128)(2,1)S(1)}, u32[]{:S(2)}, u32[]{:S(2)}) collective-permute-start(bf16[128,64]{0,1:T(8,128)(2,1)S(1)} %slice.131), channel_id=1, source_target_pairs={{0,4},{4,8},{8,12},{12,16},{16,20},{20,24},{24,28},{1,5},{5,9},{9,... | collective-permute-start | bytes 49160 | tf_op jit(solution)/shard_map/ppermute | solution.py:19
  11.8 27.8 %collective-permute-start.16 = (bf16[256,1408]{1,0:T(8,128)(2,1)}, bf16[256,1408]{1,0:T(8,128)(2,1)}, u32[]{:S(2)}, u32[]{:S(2)}) collective-permute-start(bf16[256,1408]{1,0:T(8,128)(2,1)} %refs_13_.1), channel_id=1, source_target_pairs={{0,8},{8,16},{16,24},{24,28},{28,20},{20,12},{12,4},{4,0},{1,9},{9... | collective-permute-start | bytes 2162696 | tf_op jit(solution)/shard_map/ppermute | solution.py:178
  20.1 1.6 copy-start.5
  20.2 2.4 %copy-start.8 = (bf16[768,64]{0,1:T(8,128)(2,1)S(1)}, bf16[768,64]{0,1:T(8,128)(2,1)}, u32[]{:S(2)}) copy-start(bf16[768,64]{0,1:T(8,128)(2,1)} %param.15) | copy-start | bytes 294916
  26.3 5.2 %collective-permute-start.2 = (bf16[192,256]{0,1:T(8,128)(2,1)S(1)}, bf16[192,256]{0,1:T(8,128)(2,1)S(1)}, u32[]{:S(2)}, u32[]{:S(2)}) collective-permute-start(bf16[192,256]{0,1:T(8,128)(2,1)S(1)} %get-tuple-element.19), channel_id=1, source_target_pairs={{0,1},{1,2},{2,3},{3,0},{4,5},{5,6},{6,7},{7,4},{8,9},{9,10},{10,1... | collective-permute-start | bytes 294920 | tf_op jit(solution)/shard_map/ppermute | solution.py:119
  26.3 6.4 %collective-permute-start.3 = (bf16[192,256]{0,1:T(8,128)(2,1)S(1)}, bf16[192,256]{0,1:T(8,128)(2,1)S(1)}, u32[]{:S(2)}, u32[]{:S(2)}) collective-permute-start(bf16[192,256]{0,1:T(8,128)(2,1)S(1)} %get-tuple-element.18), channel_id=1, source_target_pairs={{0,2},{1,3},{2,0},{3,1},{4,6},{5,7},{6,4},{7,5},{8,10},{9,11},{10,... | collective-permute-start | bytes 294920 | tf_op jit(solution)/shard_map/ppermute | solution.py:119
  31.4 3.8 %collective-permute-start.4 = (bf16[192,256]{0,1:T(8,128)(2,1)S(1)}, bf16[192,256]{0,1:T(8,128)(2,1)S(1)}, u32[]{:S(2)}, u32[]{:S(2)}) collective-permute-start(bf16[192,256]{0,1:T(8,128)(2,1)S(1)} %get-tuple-element.17), channel_id=1, source_target_pairs={{0,3},{1,0},{2,1},{3,2},{4,7},{5,4},{6,5},{7,6},{8,11},{9,8},{10,9... | collective-permute-start | bytes 294920 | tf_op jit(solution)/shard_map/ppermute | solution.py:119
  32.8 20.9 %collective-permute-start.17 = (bf16[256,1408]{1,0:T(8,128)(2,1)}, bf16[256,1408]{1,0:T(8,128)(2,1)}, u32[]{:S(2)}, u32[]{:S(2)}) collective-permute-start(bf16[256,1408]{1,0:T(8,128)(2,1)} %refs_13_.1), channel_id=1, source_target_pairs={{8,0},{16,8},{24,16},{28,24},{20,28},{12,20},{4,12},{0,4},{9,1},{1... | collective-permute-start | bytes 2162696 | tf_op jit(solution)/shard_map/ppermute | solution.py:179
  35.2 33.8 %collective-permute-start.25 = (bf16[1408,256]{1,0:T(8,128)(2,1)}, bf16[1408,256]{1,0:T(8,128)(2,1)}, u32[]{:S(2)}, u32[]{:S(2)}) collective-permute-start(bf16[1408,256]{1,0:T(8,128)(2,1)} %param.21), channel_id=1, source_target_pairs={{8,0},{16,8},{24,16},{28,24},{20,28},{12,20},{4,12},{0,4},{9,1},{1... | collective-permute-start | bytes 2162696 | tf_op jit(solution)/shard_map/ppermute | solution.py:179
  36.5 33.5 %collective-permute-start.24 = (bf16[1408,256]{1,0:T(8,128)(2,1)}, bf16[1408,256]{1,0:T(8,128)(2,1)}, u32[]{:S(2)}, u32[]{:S(2)}) collective-permute-start(bf16[1408,256]{1,0:T(8,128)(2,1)} %param.21), channel_id=1, source_target_pairs={{0,8},{8,16},{16,24},{24,28},{28,20},{20,12},{12,4},{4,0},{1,9},{9... | collective-permute-start | bytes 2162696 | tf_op jit(solution)/shard_map/ppermute | solution.py:178
  37.6 33.3 %collective-permute-start.10 = (bf16[256,1408]{1,0:T(8,128)(2,1)S(1)}, bf16[256,1408]{1,0:T(8,128)(2,1)S(1)}, u32[]{:S(2)}, u32[]{:S(2)}) collective-permute-start(bf16[256,1408]{1,0:T(8,128)(2,1)S(1)} %collective-permute-done.8.refs_5_), channel_id=1, source_target_pairs={{0,8},{8,16},{16,24},{24,28},{28,20},{20,12},{12,4},{4,0},{1,9},{9... | collective-permute-start | bytes 2162696 | tf_op jit(solution)/shard_map/ppermute | solution.py:178
  39.6 44.9 %collective-permute-start.11 = (bf16[256,1408]{1,0:T(8,128)(2,1)S(1)}, bf16[256,1408]{1,0:T(8,128)(2,1)}, u32[]{:S(2)}, u32[]{:S(2)}) collective-permute-start(bf16[256,1408]{1,0:T(8,128)(2,1)S(1)} %collective-permute-done.9.refs_6_), channel_id=1, source_target_pairs={{8,0},{16,8},{24,16},{28,24},{20,28},{12,20},{4,12},{0,4},{9,1},{1... | collective-permute-start | bytes 2162696 | tf_op jit(solution)/shard_map/ppermute | solution.py:179
  53.6 36.5 %collective-permute-start.18 = (bf16[256,1408]{1,0:T(8,128)(2,1)}, bf16[256,1408]{1,0:T(8,128)(2,1)S(1)}, u32[]{:S(2)}, u32[]{:S(2)}) collective-permute-start(bf16[256,1408]{1,0:T(8,128)(2,1)} %collective-permute-done.16.refs_14_), channel_id=1, source_target_pairs={{0,8},{8,16},{16,24},{24,28},{28,20},{20,12},{12,4},{4,0},{1,9},{9... | collective-permute-start | bytes 2162696 | tf_op jit(solution)/shard_map/ppermute | solution.py:178
  69.1 30.8 %collective-permute-start.19 = (bf16[256,1408]{1,0:T(8,128)(2,1)}, bf16[256,1408]{1,0:T(8,128)(2,1)S(1)}, u32[]{:S(2)}, u32[]{:S(2)}) collective-permute-start(bf16[256,1408]{1,0:T(8,128)(2,1)} %collective-permute-done.17.refs_15_), channel_id=1, source_target_pairs={{8,0},{16,8},{24,16},{28,24},{20,28},{12,20},{4,12},{0,4},{9,1},{1... | collective-permute-start | bytes 2162696 | tf_op jit(solution)/shard_map/ppermute | solution.py:179
  70.1 45.3 %collective-permute-start.30 = (bf16[1408,256]{1,0:T(8,128)(2,1)}, bf16[1408,256]{1,0:T(8,128)(2,1)S(1)}, u32[]{:S(2)}, u32[]{:S(2)}) collective-permute-start(bf16[1408,256]{1,0:T(8,128)(2,1)} %collective-permute-done.25), channel_id=1, source_target_pairs={{8,0},{16,8},{24,16},{28,24},{20,28},{12,20},{4,12},{0,4},{9,1},{1... | collective-permute-start | bytes 2162696 | tf_op jit(solution)/shard_map/ppermute | solution.py:179
  70.9 45.4 %copy-start.12 = (f32[2048]{0:T(1024)S(1)}, f32[2048]{0:T(1024)}, u32[]{:S(2)}) copy-start(f32[2048]{0:T(1024)} %param.18) | copy-start | bytes 24580
  70.9 19.2 %copy-start.1 = (bf16[256,1408]{1,0:T(8,128)(2,1)}, bf16[256,1408]{1,0:T(8,128)(2,1)S(1)}, u32[]{:S(2)}) copy-start(bf16[256,1408]{1,0:T(8,128)(2,1)S(1)} %collective-permute-done.10.refs_7_) | copy-start | bytes 2162692
  70.9 46.5 %collective-permute-start.29 = (bf16[1408,256]{1,0:T(8,128)(2,1)}, bf16[1408,256]{1,0:T(8,128)(2,1)S(1)}, u32[]{:S(2)}, u32[]{:S(2)}) collective-permute-start(bf16[1408,256]{1,0:T(8,128)(2,1)} %collective-permute-done.24), channel_id=1, source_target_pairs={{0,8},{8,16},{16,24},{24,28},{28,20},{20,12},{12,4},{4,0},{1,9},{9... | collective-permute-start | bytes 2162696 | tf_op jit(solution)/shard_map/ppermute | solution.py:178
  84.5 32.9 %collective-permute-start.12 = (bf16[256,1408]{1,0:T(8,128)(2,1)S(1)}, bf16[256,1408]{1,0:T(8,128)(2,1)S(1)}, u32[]{:S(2)}, u32[]{:S(2)}) collective-permute-start(bf16[256,1408]{1,0:T(8,128)(2,1)S(1)} %collective-permute-done.10.refs_7_), channel_id=1, source_target_pairs={{0,8},{8,16},{16,24},{24,28},{28,20},{20,12},{12,4},{4,0},{1,9},{9... | collective-permute-start | bytes 2162696 | tf_op jit(solution)/shard_map/ppermute | solution.py:178
  90.1 60.3 %copy-start.3 = (bf16[192,2048]{1,0:T(8,128)(2,1)}, bf16[192,2048]{1,0:T(8,128)(2,1)S(1)}, u32[]{:S(2)}) copy-start(bf16[192,2048]{1,0:T(8,128)(2,1)S(1)} %get-tuple-element.32) | copy-start | bytes 2359300
  90.1 73.7 %copy-start.20 = (bf16[256,1408]{1,0:T(8,128)(2,1)}, bf16[256,1408]{1,0:T(8,128)(2,1)S(1)}, u32[]{:S(2)}) copy-start(bf16[256,1408]{1,0:T(8,128)(2,1)S(1)} %collective-permute-done.18.refs_16_) | copy-start | bytes 2162692
  90.1 40.6 %collective-permute-start.13 = (bf16[256,1408]{1,0:T(8,128)(2,1)}, bf16[256,1408]{1,0:T(8,128)(2,1)S(1)}, u32[]{:S(2)}, u32[]{:S(2)}) collective-permute-start(bf16[256,1408]{1,0:T(8,128)(2,1)} %collective-permute-done.11.refs_8_), channel_id=1, source_target_pairs={{8,0},{16,8},{24,16},{28,24},{20,28},{12,20},{4,12},{0,4},{9,1},{1... | collective-permute-start | bytes 2162696 | tf_op jit(solution)/shard_map/ppermute | solution.py:179
  99.9 63.9 %copy-start.21 = (bf16[256,1408]{1,0:T(8,128)(2,1)}, bf16[256,1408]{1,0:T(8,128)(2,1)S(1)}, u32[]{:S(2)}) copy-start(bf16[256,1408]{1,0:T(8,128)(2,1)S(1)} %collective-permute-done.19.refs_17_) | copy-start | bytes 2162692
  99.9 32.6 %collective-permute-start.20 = (bf16[256,1408]{1,0:T(8,128)(2,1)S(1)}, bf16[256,1408]{1,0:T(8,128)(2,1)S(1)}, u32[]{:S(2)}, u32[]{:S(2)}) collective-permute-start(bf16[256,1408]{1,0:T(8,128)(2,1)S(1)} %collective-permute-done.18.refs_16_), channel_id=1, source_target_pairs={{0,8},{8,16},{16,24},{24,28},{28,20},{20,12},{12,4},{4,0},{1,9},{9... | collective-permute-start | bytes 2162696 | tf_op jit(solution)/shard_map/ppermute | solution.py:178
  115.3 35.1 %copy-start.16 = (bf16[1408,256]{1,0:T(8,128)(2,1)}, bf16[1408,256]{1,0:T(8,128)(2,1)S(1)}, u32[]{:S(2)}) copy-start(bf16[1408,256]{1,0:T(8,128)(2,1)S(1)} %collective-permute-done.30) | copy-start | bytes 2162692
  115.3 30.9 %collective-permute-start.21 = (bf16[256,1408]{1,0:T(8,128)(2,1)S(1)}, bf16[256,1408]{1,0:T(8,128)(2,1)S(1)}, u32[]{:S(2)}, u32[]{:S(2)}) collective-permute-start(bf16[256,1408]{1,0:T(8,128)(2,1)S(1)} %collective-permute-done.19.refs_17_), channel_id=1, source_target_pairs={{8,0},{16,8},{24,16},{28,24},{20,28},{12,20},{4,12},{0,4},{9,1},{1... | collective-permute-start | bytes 2162696 | tf_op jit(solution)/shard_map/ppermute | solution.py:179
  117.4 46.4 %copy-start.18 = (bf16[1408,256]{1,0:T(8,128)(2,1)}, bf16[1408,256]{1,0:T(8,128)(2,1)S(1)}, u32[]{:S(2)}) copy-start(bf16[1408,256]{1,0:T(8,128)(2,1)S(1)} %collective-permute-done.29) | copy-start | bytes 2162692
  117.4 33.0 %collective-permute-start.5 = (bf16[192,2048]{1,0:T(8,128)(2,1)}, bf16[192,2048]{1,0:T(8,128)(2,1)S(1)}, u32[]{:S(2)}, u32[]{:S(2)}) collective-permute-start(bf16[192,2048]{1,0:T(8,128)(2,1)} %fusion.5.refs_0_), channel_id=1, source_target_pairs={{0,1},{1,2},{2,3},{3,0},{4,5},{5,6},{6,7},{7,4},{8,9},{9,10},{10,1... | collective-permute-start | bytes 2359304 | tf_op jit(solution)/shard_map/ppermute | solution.py:119
  117.4 34.5 %collective-permute-start.6 = (bf16[192,2048]{1,0:T(8,128)(2,1)}, bf16[192,2048]{1,0:T(8,128)(2,1)S(1)}, u32[]{:S(2)}, u32[]{:S(2)}) collective-permute-start(bf16[192,2048]{1,0:T(8,128)(2,1)} %fusion.5.refs_0_), channel_id=1, source_target_pairs={{0,2},{1,3},{2,0},{3,1},{4,6},{5,7},{6,4},{7,5},{8,10},{9,11},{10,... | collective-permute-start | bytes 2359304 | tf_op jit(solution)/shard_map/ppermute | solution.py:119
  130.8 19.6 %copy-start.9 = (bf16[256,1408]{1,0:T(8,128)(2,1)}, bf16[256,1408]{1,0:T(8,128)(2,1)S(1)}, u32[]{:S(2)}) copy-start(bf16[256,1408]{1,0:T(8,128)(2,1)S(1)} %collective-permute-done.13.refs_10_) | copy-start | bytes 2162692
  130.8 31.0 %collective-permute-start.35 = (bf16[1408,256]{1,0:T(8,128)(2,1)S(1)}, bf16[1408,256]{1,0:T(8,128)(2,1)}, u32[]{:S(2)}, u32[]{:S(2)}) collective-permute-start(bf16[1408,256]{1,0:T(8,128)(2,1)S(1)} %collective-permute-done.30), channel_id=1, source_target_pairs={{8,0},{16,8},{24,16},{28,24},{20,28},{12,20},{4,12},{0,4},{9,1},{1... | collective-permute-start | bytes 2162696 | tf_op jit(solution)/shard_map/ppermute | solution.py:179
  132.5 19.4 %copy-start.10 = (bf16[256,1408]{1,0:T(8,128)(2,1)}, bf16[256,1408]{1,0:T(8,128)(2,1)S(1)}, u32[]{:S(2)}) copy-start(bf16[256,1408]{1,0:T(8,128)(2,1)S(1)} %collective-permute-done.20.refs_18_) | copy-start | bytes 2162692
  132.5 31.3 %collective-permute-start.34 = (bf16[1408,256]{1,0:T(8,128)(2,1)S(1)}, bf16[1408,256]{1,0:T(8,128)(2,1)}, u32[]{:S(2)}, u32[]{:S(2)}) collective-permute-start(bf16[1408,256]{1,0:T(8,128)(2,1)S(1)} %collective-permute-done.29), channel_id=1, source_target_pairs={{0,8},{8,16},{16,24},{24,28},{28,20},{20,12},{12,4},{4,0},{1,9},{9... | collective-permute-start | bytes 2162696 | tf_op jit(solution)/shard_map/ppermute | solution.py:178
  146.2 5.7 %copy-start.11 = (bf16[256,1408]{1,0:T(8,128)(2,1)}, bf16[256,1408]{1,0:T(8,128)(2,1)S(1)}, u32[]{:S(2)}) copy-start(bf16[256,1408]{1,0:T(8,128)(2,1)S(1)} %collective-permute-done.21.refs_19_) | copy-start | bytes 2162692
  146.2 28.1 %collective-permute-start.7 = (bf16[192,2048]{1,0:T(8,128)(2,1)}, bf16[192,2048]{1,0:T(8,128)(2,1)}, u32[]{:S(2)}, u32[]{:S(2)}) collective-permute-start(bf16[192,2048]{1,0:T(8,128)(2,1)} %fusion.5.refs_0_), channel_id=1, source_target_pairs={{0,3},{1,0},{2,1},{3,2},{4,7},{5,4},{6,5},{7,6},{8,11},{9,8},{10,9... | collective-permute-start | bytes 2359304 | tf_op jit(solution)/shard_map/ppermute | solution.py:119
  148.8 28.3 %copy-start = (bf16[256,1408]{1,0:T(8,128)(2,1)S(1)}, bf16[256,1408]{1,0:T(8,128)(2,1)}, u32[]{:S(2)}) copy-start(bf16[256,1408]{1,0:T(8,128)(2,1)} %refs_4_.1) | copy-start | bytes 2162692
  150.4 2.2 copy-start.14
  150.4 26.0 %collective-permute-start.14 = (bf16[128,1408]{1,0:T(8,128)(2,1)}, bf16[128,1408]{1,0:T(8,128)(2,1)S(1)}, u32[]{:S(2)}, u32[]{:S(2)}) collective-permute-start(bf16[128,1408]{1,0:T(8,128)(2,1)} %slice.172), channel_id=1, source_target_pairs={{0,8},{8,16},{16,24},{24,28},{28,20},{20,12},{12,4},{4,0},{1,9},{9... | collective-permute-start | bytes 1081352 | tf_op jit(solution)/shard_map/ppermute | solution.py:182
  151.9 9.8 %copy-start.15 = (bf16[192,2048]{1,0:T(8,128)(2,1)}, bf16[192,2048]{1,0:T(8,128)(2,1)S(1)}, u32[]{:S(2)}) copy-start(bf16[192,2048]{1,0:T(8,128)(2,1)S(1)} %collective-permute-done.6.refs_2_) | copy-start | bytes 2359300
  151.9 24.5 %collective-permute-start.15 = (bf16[128,1408]{1,0:T(8,128)(2,1)}, bf16[128,1408]{1,0:T(8,128)(2,1)}, u32[]{:S(2)}, u32[]{:S(2)}) collective-permute-start(bf16[128,1408]{1,0:T(8,128)(2,1)} %slice.173), channel_id=1, source_target_pairs={{8,0},{16,8},{24,16},{28,24},{20,28},{12,20},{4,12},{0,4},{9,1},{1... | collective-permute-start | bytes 1081352 | tf_op jit(solution)/shard_map/ppermute | solution.py:183
  161.8 14.7 %collective-permute-start.22 = (bf16[128,1408]{1,0:T(8,128)(2,1)}, bf16[128,1408]{1,0:T(8,128)(2,1)}, u32[]{:S(2)}, u32[]{:S(2)}) collective-permute-start(bf16[128,1408]{1,0:T(8,128)(2,1)} %slice.174), channel_id=1, source_target_pairs={{0,8},{8,16},{16,24},{24,28},{28,20},{20,12},{12,4},{4,0},{1,9},{9... | collective-permute-start | bytes 1081352 | tf_op jit(solution)/shard_map/ppermute | solution.py:182
  163.8 13.3 %collective-permute-start.23 = (bf16[128,1408]{1,0:T(8,128)(2,1)}, bf16[128,1408]{1,0:T(8,128)(2,1)}, u32[]{:S(2)}, u32[]{:S(2)}) collective-permute-start(bf16[128,1408]{1,0:T(8,128)(2,1)} %slice.175), channel_id=1, source_target_pairs={{8,0},{16,8},{24,16},{28,24},{20,28},{12,20},{4,12},{0,4},{9,1},{1... | collective-permute-start | bytes 1081352 | tf_op jit(solution)/shard_map/ppermute | solution.py:183
  170.4 6.7 %copy-start.2 = (bf16[256,1408]{1,0:T(8,128)(2,1)S(1)}, bf16[256,1408]{1,0:T(8,128)(2,1)}, u32[]{:S(2)}) copy-start(bf16[256,1408]{1,0:T(8,128)(2,1)} %copy-done.1) | copy-start | bytes 2162692
  174.3 35.1 %collective-permute-start.39 = (bf16[704,256]{1,0:T(8,128)(2,1)S(1)}, bf16[704,256]{1,0:T(8,128)(2,1)S(1)}, u32[]{:S(2)}, u32[]{:S(2)}) collective-permute-start(bf16[704,256]{1,0:T(8,128)(2,1)S(1)} %slice.199), channel_id=1, source_target_pairs={{0,8},{8,16},{16,24},{24,28},{28,20},{20,12},{12,4},{4,0},{1,9},{9... | collective-permute-start | bytes 1081352 | tf_op jit(solution)/shard_map/ppermute | solution.py:182
  176.4 33.1 %collective-permute-start.40 = (bf16[704,256]{1,0:T(8,128)(2,1)S(1)}, bf16[704,256]{1,0:T(8,128)(2,1)S(1)}, u32[]{:S(2)}, u32[]{:S(2)}) collective-permute-start(bf16[704,256]{1,0:T(8,128)(2,1)S(1)} %slice.200), channel_id=1, source_target_pairs={{8,0},{16,8},{24,16},{28,24},{20,28},{12,20},{4,12},{0,4},{9,1},{1... | collective-permute-start | bytes 1081352 | tf_op jit(solution)/shard_map/ppermute | solution.py:183
  193.0 2.7 %copy-start.22 = (bf16[768,1408]{1,0:T(8,128)(2,1)S(1)}, bf16[768,1408]{1,0:T(8,128)(2,1)}, u32[]{:S(2)}) copy-start(bf16[768,1408]{1,0:T(8,128)(2,1)} %shard_map.118) | copy-start | bytes 6488068
  199.5 11.4 %collective-permute-start.36 = (bf16[192,512]{1,0:T(8,128)(2,1)S(1)}, bf16[192,512]{1,0:T(8,128)(2,1)S(1)}, u32[]{:S(2)}, u32[]{:S(2)}) collective-permute-start(bf16[192,512]{1,0:T(8,128)(2,1)S(1)} %get-tuple-element.8), channel_id=1, source_target_pairs={{0,1},{1,2},{2,3},{3,0},{4,5},{5,6},{6,7},{7,4},{8,9},{9,10},{10,1... | collective-permute-start | bytes 589832 | tf_op jit(solution)/shard_map/ppermute | solution.py:119
  199.6 12.8 %collective-permute-start.37 = (bf16[192,512]{1,0:T(8,128)(2,1)S(1)}, bf16[192,512]{1,0:T(8,128)(2,1)S(1)}, u32[]{:S(2)}, u32[]{:S(2)}) collective-permute-start(bf16[192,512]{1,0:T(8,128)(2,1)S(1)} %get-tuple-element.10), channel_id=1, source_target_pairs={{0,2},{1,3},{2,0},{3,1},{4,6},{5,7},{6,4},{7,5},{8,10},{9,11},{10,... | collective-permute-start | bytes 589832 | tf_op jit(solution)/shard_map/ppermute | solution.py:119
  201.1 11.2 %collective-permute-start.38 = (bf16[192,512]{1,0:T(8,128)(2,1)S(1)}, bf16[192,512]{1,0:T(8,128)(2,1)S(1)}, u32[]{:S(2)}, u32[]{:S(2)}) collective-permute-start(bf16[192,512]{1,0:T(8,128)(2,1)S(1)} %get-tuple-element.9), channel_id=1, source_target_pairs={{0,3},{1,0},{2,1},{3,2},{4,7},{5,4},{6,5},{7,6},{8,11},{9,8},{10,9... | collective-permute-start | bytes 589832 | tf_op jit(solution)/shard_map/ppermute | solution.py:119
  209.4 6.6 %collective-permute-start.31 = (bf16[192,512]{1,0:T(8,128)(2,1)S(1)}, bf16[192,512]{1,0:T(8,128)(2,1)S(1)}, u32[]{:S(2)}, u32[]{:S(2)}) collective-permute-start(bf16[192,512]{1,0:T(8,128)(2,1)S(1)} %get-tuple-element.11), channel_id=1, source_target_pairs={{0,1},{1,2},{2,3},{3,0},{4,5},{5,6},{6,7},{7,4},{8,9},{9,10},{10,1... | collective-permute-start | bytes 589832 | tf_op jit(solution)/shard_map/ppermute | solution.py:119
  209.5 7.8 %collective-permute-start.32 = (bf16[192,512]{1,0:T(8,128)(2,1)S(1)}, bf16[192,512]{1,0:T(8,128)(2,1)S(1)}, u32[]{:S(2)}, u32[]{:S(2)}) collective-permute-start(bf16[192,512]{1,0:T(8,128)(2,1)S(1)} %get-tuple-element.13), channel_id=1, source_target_pairs={{0,2},{1,3},{2,0},{3,1},{4,6},{5,7},{6,4},{7,5},{8,10},{9,11},{10,... | collective-permute-start | bytes 589832 | tf_op jit(solution)/shard_map/ppermute | solution.py:119
  210.9 9.1 %collective-permute-start.33 = (bf16[192,512]{1,0:T(8,128)(2,1)S(1)}, bf16[192,512]{1,0:T(8,128)(2,1)S(1)}, u32[]{:S(2)}, u32[]{:S(2)}) collective-permute-start(bf16[192,512]{1,0:T(8,128)(2,1)S(1)} %get-tuple-element.12), channel_id=1, source_target_pairs={{0,3},{1,0},{2,1},{3,2},{4,7},{5,4},{6,5},{7,6},{8,11},{9,8},{10,9... | collective-permute-start | bytes 589832 | tf_op jit(solution)/shard_map/ppermute | solution.py:119
  212.4 14.2 %collective-permute-start.26 = (bf16[192,768]{1,0:T(8,128)(2,1)S(1)}, bf16[192,768]{1,0:T(8,128)(2,1)S(1)}, u32[]{:S(2)}, u32[]{:S(2)}) collective-permute-start(bf16[192,768]{1,0:T(8,128)(2,1)S(1)} %get-tuple-element.5), channel_id=1, source_target_pairs={{0,1},{1,2},{2,3},{3,0},{4,5},{5,6},{6,7},{7,4},{8,9},{9,10},{10,1... | collective-permute-start | bytes 884744 | tf_op jit(solution)/shard_map/ppermute | solution.py:119
  212.4 15.5 %collective-permute-start.27 = (bf16[192,768]{1,0:T(8,128)(2,1)S(1)}, bf16[192,768]{1,0:T(8,128)(2,1)S(1)}, u32[]{:S(2)}, u32[]{:S(2)}) collective-permute-start(bf16[192,768]{1,0:T(8,128)(2,1)S(1)} %get-tuple-element.7), channel_id=1, source_target_pairs={{0,2},{1,3},{2,0},{3,1},{4,6},{5,7},{6,4},{7,5},{8,10},{9,11},{10,... | collective-permute-start | bytes 884744 | tf_op jit(solution)/shard_map/ppermute | solution.py:119
  216.0 16.2 %collective-permute-start.28 = (bf16[192,768]{1,0:T(8,128)(2,1)S(1)}, bf16[192,768]{1,0:T(8,128)(2,1)S(1)}, u32[]{:S(2)}, u32[]{:S(2)}) collective-permute-start(bf16[192,768]{1,0:T(8,128)(2,1)S(1)} %get-tuple-element.6), channel_id=1, source_target_pairs={{0,3},{1,0},{2,1},{3,2},{4,7},{5,4},{6,5},{7,6},{8,11},{9,8},{10,9... | collective-permute-start | bytes 884744 | tf_op jit(solution)/shard_map/ppermute | solution.py:119
  216.1 16.3 %copy-start.4 = (bf16[192,2048]{1,0:T(8,128)(2,1)S(1)}, bf16[192,2048]{1,0:T(8,128)(2,1)}, u32[]{:S(2)}) copy-start(bf16[192,2048]{1,0:T(8,128)(2,1)} %copy-done.3) | copy-start | bytes 2359300
  217.4 17.6 %collective-permute-start.41 = (bf16[192,256]{1,0:T(8,128)(2,1)S(1)}, bf16[192,256]{1,0:T(8,128)(2,1)S(1)}, u32[]{:S(2)}, u32[]{:S(2)}) collective-permute-start(bf16[192,256]{1,0:T(8,128)(2,1)S(1)} %get-tuple-element.14), channel_id=1, source_target_pairs={{0,1},{1,2},{2,3},{3,0},{4,5},{5,6},{6,7},{7,4},{8,9},{9,10},{10,1... | collective-permute-start | bytes 294920 | tf_op jit(solution)/shard_map/ppermute | solution.py:119
  220.1 16.3 %collective-permute-start.42 = (bf16[192,256]{1,0:T(8,128)(2,1)S(1)}, bf16[192,256]{1,0:T(8,128)(2,1)S(1)}, u32[]{:S(2)}, u32[]{:S(2)}) collective-permute-start(bf16[192,256]{1,0:T(8,128)(2,1)S(1)} %get-tuple-element.16), channel_id=1, source_target_pairs={{0,2},{1,3},{2,0},{3,1},{4,6},{5,7},{6,4},{7,5},{8,10},{9,11},{10,... | collective-permute-start | bytes 294920 | tf_op jit(solution)/shard_map/ppermute | solution.py:119
  226.6 9.8 %collective-permute-start.43 = (bf16[192,256]{1,0:T(8,128)(2,1)S(1)}, bf16[192,256]{1,0:T(8,128)(2,1)S(1)}, u32[]{:S(2)}, u32[]{:S(2)}) collective-permute-start(bf16[192,256]{1,0:T(8,128)(2,1)S(1)} %get-tuple-element.15), channel_id=1, source_target_pairs={{0,3},{1,0},{2,1},{3,2},{4,7},{5,4},{6,5},{7,6},{8,11},{9,8},{10,9... | collective-permute-start | bytes 294920 | tf_op jit(solution)/shard_map/ppermute | solution.py:119
  232.7 3.6 %copy-start.6 = (bf16[192,2048]{1,0:T(8,128)(2,1)}, bf16[192,2048]{1,0:T(8,128)(2,1)S(1)}, u32[]{:S(2)}) copy-start(bf16[192,2048]{1,0:T(8,128)(2,1)S(1)} %fusion.47) | copy-start | bytes 2359300
  (3 other events, 3.0 us)
